TPU v7x, 512 devices: a whole 4x4x16 slice. The times are simulated.
512 devices in a mesh: sp: 32 (over z, core), tp: 16 (over y, x).
Axes of the slice: x: 4, y: 4, z: 16, core: 2. Of those that a mesh axis runs over, the one named last changes fastest.
Arguments:
- query_a: bfloat16 [6144, 2048], P('sp', 'tp'), may hold values from -6 to 6
- key_a: bfloat16 [6144, 2048], P('sp', 'tp'), may hold values from -6 to 6
- value_a: bfloat16 [6144, 2048], P('sp', 'tp'), may hold values from -6 to 6
- query_b: bfloat16 [6144, 2048], P('sp', 'tp'), may hold values from -6 to 6
- key_b: bfloat16 [6144, 2048], P('sp', 'tp'), may hold values from -6 to 6
- value_b: bfloat16 [6144, 2048], P('sp', 'tp'), may hold values from -6 to 6
- stop_a: float32 [6144, 32], P('sp', 'tp'), may hold values from -14 to -1
- stop_b: float32 [6144, 16], P('sp', 'tp'), may hold values from -14 to -1
- out_a: bfloat16 [2048, 2048], P('tp'), may hold values from -4 to 4
- out_b: bfloat16 [2048, 2048], P('tp'), may hold values from -4 to 4
- resid: bfloat16 [6144, 2048], P('sp', 'tp'), may hold values from -20 to 20
- mix_gain: float32 [2048], P('tp'), may hold values from 0.1 to 1.9
- ffn_gain: float32 [2048], P('tp'), may hold values from 0.1 to 1.9
- routes: int32 [6144, 2], P('sp'), may hold values from 0 to 127, all different within a row; in each aligned block of 192 rows (0 to 191, 192 to 383, ...) at most 5 rows name the same one
- gates: float32 [6144, 2], P('sp'), may hold values from 0.25 to 1.5
- exp_gate: bfloat16 [128, 2048, 512], P('sp', 'tp'), may hold values from -0.125 to 0.125
- exp_up: bfloat16 [128, 2048, 512], P('sp', 'tp'), may hold values from -0.125 to 0.125
- exp_down: bfloat16 [128, 512, 2048], P('sp', None, 'tp'), may hold values from -0.25 to 0.25
- sh_gate: bfloat16 [2048, 512], P('tp'), may hold values from -0.125 to 0.125
- sh_up: bfloat16 [2048, 512], P('tp'), may hold values from -0.125 to 0.125
- sh_down: bfloat16 [512, 2048], P(None, 'tp'), may hold values from -4 to 4
Outputs:
- result: bfloat16 [6144, 2048], P('sp', 'tp')
Inputs may be any that keep to these rules, and one draw needn't show every extreme that they name: `routes`: each row names 2 different experts. Within the rows of one index of sp (aligned blocks of 192 rows) no expert is named by more than 5 rows, a bound that some block reaches.
All inputs are finite; a program needn't handle non-finite values.
Results may differ from a plain program's by a relative error of at most 0.02.
Values may be sent and summed in bfloat16 or wider, within the bound.
A program may use at most 64 MiB of HBM per device.

v0:
```python
import jax
import jax.numpy as jnp
from jax import lax
from jax.sharding import Mesh
from jax.sharding import PartitionSpec as P

D = 2048
TP = ("tp_0", "tp_1")


epsilon = 1e-06


def cut_along(x, dim, size):
    before, after = (x.shape[:dim], x.shape[dim + 1 :])
    return jnp.moveaxis(x.reshape(*before, size, -1, *after), dim, 0)


def sum_at_owner(x, axis, dim):
    tiles = cut_along(x, dim, lax.axis_size(axis))
    arrived = lax.all_to_all(tiles, axis, split_axis=0, concat_axis=0, tiled=True)
    return arrived.astype(jnp.float32).sum(axis=0)


def by_axis(x, axes):
    for axis in axes:
        x = lax.psum(x, axis)
    return x


def suffix_sums(failing):
    width = failing.shape[-1]
    pieces = width // width
    shaped = failing.reshape(failing.shape[:-1] + (pieces, width))
    places = jnp.arange(width)
    upper = (places[:, None] > places[None, :]).astype(jnp.float32)
    inner = jnp.matmul(shaped, upper)
    return inner.reshape(failing.shape)


def stick_block(state, queries, keyset, causal):
    outputs, carried = state
    new_out = []
    new_carry = []
    for group in range(2):
        query, stop, scale = queries[group]
        keys = keyset[2 * group]
        values = keyset[2 * group + 1]
        scores = jnp.einsum("qhd,khd->hqk", query, keys, preferred_element_type=jnp.float32)
        scores = scores * scale + jnp.transpose(stop)[:, :, None]
        failing = jax.nn.log_sigmoid(-scores)
        if causal is not None:
            failing = jnp.where(causal, failing, 0.0)
        after = suffix_sums(failing) + carried[group][:, :, None]
        weight = jnp.exp(jax.nn.log_sigmoid(scores) + after)
        if causal is not None:
            weight = jnp.where(causal, weight, 0.0)
        added = jnp.einsum(
            "hqk,khe->qhe", weight.astype(jnp.bfloat16), values, preferred_element_type=jnp.float32
        )
        new_out.append(outputs[group] + added)
        new_carry.append(carried[group] + jnp.sum(failing, axis=-1))
    return (tuple(new_out), tuple(new_carry))


def empty_state(count, heads_a, size_a, heads_b, size_b):
    return (
        (
            jnp.zeros((count, heads_a, size_a), jnp.float32),
            jnp.zeros((count, heads_b, size_b), jnp.float32),
        ),
        (jnp.zeros((heads_a, count), jnp.float32), jnp.zeros((heads_b, count), jnp.float32)),
    )


def joined_rows(state, width_a, width_b):
    count = state[0][0].shape[0]
    return jnp.concatenate(
        [
            state[0][0].astype(jnp.bfloat16).reshape(count, width_a),
            state[0][1].astype(jnp.bfloat16).reshape(count, width_b),
        ],
        axis=1,
    )


def shards(
    query_a,
    key_a,
    value_a,
    query_b,
    key_b,
    value_b,
    stop_a,
    stop_b,
    out_a,
    out_b,
    resid,
    mix_gain,
    ffn_gain,
    routes,
    gates,
    exp_gate,
    exp_up,
    exp_down,
    sh_gate,
    sh_up,
    sh_down,
):
    rows = query_a.shape[0]
    heads_a = stop_a.shape[1]
    heads_b = stop_b.shape[1]
    width_a = query_a.shape[1]
    width_b = query_b.shape[1]
    size_a = width_a // heads_a
    size_b = width_b // heads_b

    def unpack(joined):
        count = joined.shape[0]
        return (
            joined[:, :width_a].reshape(count, heads_a, size_a),
            joined[:, width_a : 2 * width_a].reshape(count, heads_a, size_a),
            joined[:, 2 * width_a : 2 * width_a + width_b].reshape(count, heads_b, size_b),
            joined[:, 2 * width_a + width_b :].reshape(count, heads_b, size_b),
        )

    joined_local = jnp.concatenate([key_a, value_a, key_b, value_b], axis=1)
    places = jnp.arange(rows)
    position = lax.axis_index("sp")
    n_sp = lax.axis_size("sp")
    count = query_a.shape[0]
    queries = (
        (query_a.reshape(count, heads_a, size_a), stop_a, size_a ** (-0.5)),
        (query_b.reshape(count, heads_b, size_b), stop_b, size_b ** (-0.5)),
    )
    causal = (places[None, :] < places[:, None])[None]
    state = stick_block(
        empty_state(rows, heads_a, size_a, heads_b, size_b), queries, unpack(joined_local), causal
    )
    gathered = lax.all_gather(joined_local, "sp", axis=0, tiled=True)

    def turn(step, inner_state):
        start = jnp.maximum(position - step, 0) * rows
        piece = lax.dynamic_slice_in_dim(gathered, start, rows, 0)
        return lax.cond(
            position >= step,
            lambda inputs: stick_block(inputs, queries, unpack(piece), None),
            lambda inputs: inputs,
            inner_state,
        )

    state = lax.fori_loop(1, n_sp, turn, state)
    attended = joined_rows(state, width_a, width_b)
    attended_a = attended[:, :width_a]
    attended_b = attended[:, width_a:]
    partial_value = jnp.dot(attended_a, out_a, preferred_element_type=jnp.float32)
    partial_value = partial_value + jnp.dot(attended_b, out_b, preferred_element_type=jnp.float32)
    mixed = sum_at_owner(partial_value.astype(jnp.bfloat16), TP, 1)
    mix_total = by_axis(jnp.sum(mixed * mixed, axis=1), TP)
    branch = mixed * lax.rsqrt(mix_total / D + epsilon)[:, None] * mix_gain[None, :]
    stream = lax.optimization_barrier((resid.astype(jnp.float32) + branch).astype(jnp.bfloat16))
    stream_f = stream.astype(jnp.float32)
    ffn_total = by_axis(jnp.sum(stream_f * stream_f, axis=1), TP)
    normed = (stream_f * lax.rsqrt(ffn_total / D + epsilon)[:, None] * ffn_gain[None, :]).astype(
        jnp.bfloat16
    )
    shared_gate, shared_up = (
        lax.psum(
            jnp.dot(normed, sh_gate, preferred_element_type=jnp.float32).astype(jnp.bfloat16), TP
        ).astype(jnp.float32),
        lax.psum(
            jnp.dot(normed, sh_up, preferred_element_type=jnp.float32).astype(jnp.bfloat16), TP
        ).astype(jnp.float32),
    )
    shared_hidden = (jax.nn.silu(shared_gate) * shared_up).astype(jnp.bfloat16)
    shared_out = jnp.dot(shared_hidden, sh_down, preferred_element_type=jnp.float32)
    local_experts = exp_gate.shape[0]
    experts = local_experts * n_sp
    top_count = routes.shape[1]
    capacity = max(1, (3 * rows * top_count + 2 * experts - 1) // (2 * experts))
    flat_routes = routes.reshape(-1)
    onehot = (flat_routes[:, None] == jnp.arange(experts, dtype=jnp.int32)[None, :]).astype(
        jnp.int32
    )
    earlier = jnp.cumsum(onehot, axis=0) - onehot
    slot = flat_routes * capacity + jnp.sum(earlier * onehot, axis=1)
    chooser = (slot[:, None] == jnp.arange(experts * capacity, dtype=jnp.int32)[None, :]).astype(
        jnp.bfloat16
    )
    chooser = jnp.sum(chooser.reshape(rows, top_count, experts * capacity), axis=1)
    outgoing = jnp.einsum("rs,rc->sc", chooser, normed, preferred_element_type=jnp.float32).astype(
        jnp.bfloat16
    )
    outgoing = outgoing.reshape(n_sp, local_experts, capacity, normed.shape[1])
    arrived = lax.all_to_all(outgoing, "sp", split_axis=0, concat_axis=0, tiled=True)
    gate_part = jnp.einsum("segd,edf->segf", arrived, exp_gate, preferred_element_type=jnp.float32)
    up_part = jnp.einsum("segd,edf->segf", arrived, exp_up, preferred_element_type=jnp.float32)
    gate_pre = lax.psum(gate_part.astype(jnp.bfloat16), TP).astype(jnp.float32)
    up_pre = lax.psum(up_part.astype(jnp.bfloat16), TP).astype(jnp.float32)
    hidden = (jax.nn.silu(gate_pre) * up_pre).astype(jnp.bfloat16)
    produced = jnp.einsum("segf,efd->segd", hidden, exp_down, preferred_element_type=jnp.float32)
    returned = lax.all_to_all(
        produced.astype(jnp.bfloat16), "sp", split_axis=0, concat_axis=0, tiled=True
    )
    flat_back = returned.reshape(experts * capacity, returned.shape[3])
    picked = jnp.take(flat_back, slot, axis=0).reshape(rows, top_count, returned.shape[3])
    routed = jnp.sum(gates[:, :, None] * picked.astype(jnp.float32), axis=1)
    moe = routed + shared_out
    result = stream_f + moe
    return result.astype(jnp.bfloat16)


def solution(mesh):
    finer = Mesh(mesh.devices.reshape(mesh.shape["sp"], 4, 4), ("sp", "tp_0", "tp_1"))
    in_specs = (
        P("sp", TP),
        P("sp", TP),
        P("sp", TP),
        P("sp", TP),
        P("sp", TP),
        P("sp", TP),
        P("sp", TP),
        P("sp", TP),
        P(TP, None),
        P(TP, None),
        P("sp", TP),
        P(TP),
        P(TP),
        P("sp", None),
        P("sp", None),
        P("sp", TP, None),
        P("sp", TP, None),
        P("sp", None, TP),
        P(TP, None),
        P(TP, None),
        P(None, TP),
    )
    out_specs = P("sp", TP)
    return jax.shard_map(
        shards, mesh=finer, in_specs=in_specs, out_specs=out_specs, check_vma=False
    )
```

profile of v0, /device:TPU:1, one launch (start us, length us, event | category | flops | bytes accessed | tf_op | source)
XLA Modules:
  0.0 487.4 jit_solution(6028487693172046048)
XLA Ops:
  6.5 1.6 pad_maximum_fusion
  8.2 0.9 copy.128
  9.1 0.9 copy.131
  10.0 0.9 copy.127
  10.9 0.8 copy.137
  11.7 0.1 eq.40
  11.9 0.1 copy.139
  12.0 1.1 fusion.127
  13.2 0.5 fusion.75
  13.7 0.3 fusion.133
  14.0 0.3 fusion.98
  14.3 0.2 fusion.99
  14.5 0.8 fusion.73
  15.3 76.1 %all-gather.2.cloned.1.call-done = bf16[6144,512]{1,0:T(8,128)(2,1)} async-done(((bf16[192,512]{1,0:T(8,128)(2,1)}), bf16[6144,512]{1,0:T(8,128)(2,1)}) %all-gather.2.cloned.1.call-update) | async-done | bytes 6291472 | tf_op jit(solution)/shard_map/all_gather | solution.py:140
  91.4 8.7 %copy.134 = bf16[6144,512]{0,1:T(8,128)(2,1)} copy(bf16[6144,512]{1,0:T(8,128)(2,1)} %all-gather.2.cloned.1.call-done) | data formatting | bytes 12582912 | tf_op jit(solution)/shard_map/while | solution.py:152
  100.1 6.4 %while.19 = (s32[]{:T(128)}, f32[192,2,64]{0,2,1:T(8,128)S(1)}, f32[192,1,128]{2,0,1:T(8,128)S(1)}, f32[2,192]{1,0:T(2,128)S(1)}, f32[1,192]{1,0:T(1,128)S(1)}, ...) while((s32[]{:T(128)}, f32[192,2,64]{0,2,1:T(8,128)S(1)}, ...), condition=%wide.region_7.8_spmd, body=%wide.region_2.7_spmd.sunk | while | flops 83325512 | bytes 2064037 | solution.py:152
  100.1 5.1 %conditional.2 = ((f32[192,2,64]{0,2,1:T(8,128)S(1)}, f32[192,1,128]{2,0,1:T(8,128)S(1)}, f32[2,192]{1,0:T(2,128)S(1)}, f32[1,192]{1,0:T(1,128)S(1)})) conditional(s32[]{:T(128)} %convert_element_type.258, (f32[192,2,64]{0,2,1:T(8,128)S(1)}, f32[192,1,128]{2,0,1:T(8,128)S(1)}, f32[2,192]{1,0:T(2,128)S(1)}, f32[1,192]{1,0:T(1,128)S(1)}) %tuple.58, ...), branch_computations={%region_3.3_spmd, %region_4.6_spmd} | conditional | flops 83325512 | bytes 2063786 | solution.py:145
  100.1 1.1 constant_dynamic-slice_fusion
  101.1 0.5 fusion.25
  101.6 0.7 fusion.12
  102.4 1.3 fusion.43
  103.7 1.5 fusion.13
  106.5 0.4 fusion.154
  106.9 0.6 copy-done.1
  107.5 0.4 fusion.60
  107.9 1.1 copy.166
  109.0 6.7 %all-to-all-start = ((bf16[16,192,128]{2,1,0:T(8,128)(2,1)}), bf16[16,192,128]{2,1,0:T(8,128)(2,1)S(1)}, u32[]{:S(2)}, u32[]{:S(2)}) async-start(bf16[16,192,128]{2,1,0:T(8,128)(2,1)} %bitcast.107), calls=%async_computation | async-start | bytes 1572864 | tf_op jit(solution)/shard_map/all_to_all | solution.py:21
  115.7 0.1 reshape.279
  116.0 0.2 fusion.108
  116.2 0.1 reduce_sum.108
  116.4 0.1 copy.141
  116.5 0.2 fusion.83
  116.6 9.7 %all-to-all-done = bf16[16,192,128]{2,1,0:T(8,128)(2,1)S(1)} async-done(((bf16[16,192,128]{2,1,0:T(8,128)(2,1)}), bf16[16,192,128]{2,1,0:T(8,128)(2,1)S(1)}, u32[]{:S(2)}, u32[]{:S(2)}) %all-to-all-start) | async-done | bytes 786464 | tf_op jit(solution)/shard_map/all_to_all | solution.py:21
  126.3 0.1 convert_reduce_fusion
  126.5 0.1 multiply_reduce_fusion.1
  126.6 6.5 %psum.56 = f32[192]{0:T(256)S(1)} all-reduce(f32[192]{0:T(256)S(1)} %multiply_reduce_fusion.1), channel_id=1, replica_groups=mesh['sp'=32,'tp_0'=4,'tp_1'=4] {'tp_0'}, use_global_device_ids=true, to_apply=%region_10.11 | all-reduce | flops 192 | bytes 1536 | tf_op jit(solution)/shard_map/psum | solution.py:27
  133.1 6.8 %psum.57 = f32[192]{0:T(256)S(1)} all-reduce(f32[192]{0:T(256)S(1)} %psum.56), channel_id=1, replica_groups=mesh['sp'=32,'tp_0'=4,'tp_1'=4] {'tp_1'}, use_global_device_ids=true, to_apply=%region_11.12 | all-reduce | flops 192 | bytes 1536 | tf_op jit(solution)/shard_map/psum | solution.py:27
  139.9 0.1 add_convert_fusion
  140.0 0.1 fusion.130
  140.1 6.5 %psum.58 = f32[192]{0:T(256)S(1)} all-reduce(f32[192]{0:T(256)S(1)} %fusion.130), channel_id=1, replica_groups=mesh['sp'=32,'tp_0'=4,'tp_1'=4] {'tp_0'}, use_global_device_ids=true, to_apply=%region_17.18 | all-reduce | flops 192 | bytes 1536 | tf_op jit(solution)/shard_map/psum | solution.py:27
  146.6 7.1 %psum.59 = f32[192]{0:T(256)S(1)} all-reduce(f32[192]{0:T(256)S(1)} %psum.58), channel_id=1, replica_groups=mesh['sp'=32,'tp_0'=4,'tp_1'=4] {'tp_1'}, use_global_device_ids=true, to_apply=%region_18.19 | all-reduce | flops 192 | bytes 1536 | tf_op jit(solution)/shard_map/psum | solution.py:27
  153.7 0.3 convolution_convert_fusion.5
  154.1 0.1 reshape.281
  154.1 0.7 copy.143
  154.9 161.9 %all-to-all-start.1 = ((bf16[32,4,5,128]{3,1,2,0:T(4,128)(2,1)}), bf16[32,4,5,128]{3,1,2,0:T(4,128)(2,1)S(1)}, u32[]{:S(2)}, u32[]{:S(2)}) async-start(bf16[32,4,5,128]{3,1,2,0:T(4,128)(2,1)} %copy.143), calls=%async_computation.1 | async-start | bytes 327680 | tf_op jit(solution)/shard_map/all_to_all | solution.py:195
  316.8 0.9 convolution_convert_fusion.3
  317.7 0.9 convolution_convert_fusion.2
  318.7 15.2 %all-to-all-done.1 = bf16[32,4,5,128]{3,1,2,0:T(4,128)(2,1)S(1)} async-done(((bf16[32,4,5,128]{3,1,2,0:T(4,128)(2,1)}), bf16[32,4,5,128]{3,1,2,0:T(4,128)(2,1)S(1)}, u32[]{:S(2)}, u32[]{:S(2)}) %all-to-all-start.1) | async-done | bytes 163872 | tf_op jit(solution)/shard_map/all_to_all | solution.py:195
  333.9 1.2 fusion.61
  335.0 1.2 fusion.62
  336.2 106.3 %all-reduce.3.cloned.1.call-done = (bf16[32,4,5,512]{3,0,2,1:T(8,128)(2,1)}, bf16[32,4,5,512]{3,0,2,1:T(8,128)(2,1)}, bf16[192,512]{1,0:T(8,128)(2,1)}, bf16[192,512]{1,0:T(8,128)(2,1)}) async-done(((bf16[32,4,5,512]{3,0,2,1:T(8,128)(2,1)}, bf16[32,4,5,512]{3,0,2,1:T(8,128)(2,1)}, bf16[192,512]{1,0:T(8,128)(2,1)}, bf16[192,512]{1,0:T(8,128)(2,1)}), (bf16[32,4,5,512]{3,0,2,1:T(8,128)(2,1)}, ...) | async-done | bytes 1703952 | tf_op jit(solution)/shard_map/psum | solution.py:199
  442.6 1.8 fusion.71
  444.5 0.7 copy.146
  445.2 14.6 %all-to-all-start.2 = ((bf16[32,4,5,128]{3,1,2,0:T(4,128)(2,1)}), bf16[32,4,5,128]{3,1,2,0:T(4,128)(2,1)S(1)}, u32[]{:S(2)}, u32[]{:S(2)}) async-start(bf16[32,4,5,128]{3,1,2,0:T(4,128)(2,1)} %copy.146), calls=%async_computation.2 | async-start | bytes 327680 | tf_op jit(solution)/shard_map/all_to_all | solution.py:202
  459.8 0.1 copy.148
  460.0 0.1 mul.135
  460.1 0.2 copy.142
  460.3 0.1 copy.136
  460.5 16.5 %all-to-all-done.2 = bf16[32,4,5,128]{3,1,2,0:T(4,128)(2,1)S(1)} async-done(((bf16[32,4,5,128]{3,1,2,0:T(4,128)(2,1)}), bf16[32,4,5,128]{3,1,2,0:T(4,128)(2,1)S(1)}, u32[]{:S(2)}, u32[]{:S(2)}) %all-to-all-start.2) | async-done | bytes 163872 | tf_op jit(solution)/shard_map/all_to_all | solution.py:202
  477.0 0.1 copy.147
  477.0 0.1 reshape.282
  477.1 1.4 gather_fusion
  478.6 1.1 multiply_reduce_fusion
  479.7 0.9 fusion.77
  (86 shorter events, 0.8 us)
Async XLA Ops:
  6.5 100.0 %copy-start = (bf16[128,2048]{1,0:T(8,128)(2,1)S(1)}, bf16[128,2048]{1,0:T(8,128)(2,1)}, u32[]{:S(2)}) copy-start(bf16[128,2048]{1,0:T(8,128)(2,1)} %param.33) | copy-start | bytes 1572868
  6.5 6.6 %copy-start.6 = (bf16[192,128]{1,0:T(8,128)(2,1)S(1)}, bf16[192,128]{1,0:T(8,128)(2,1)}, u32[]{:S(2)}) copy-start(bf16[192,128]{1,0:T(8,128)(2,1)} %param.30) | copy-start | bytes 147460
  6.5 84.8 %all-gather.2.cloned.1.call-start = ((), (), s32[]{:S(2)}) async-start(), calls=%async_computation.3 | async-start | bytes 6488064 | tf_op jit(solution)/shard_map/all_gather | solution.py:140
  8.2 5.5 %copy-start.10 = (f32[192,2]{0,1:T(2,128)S(1)}, f32[192,2]{0,1:T(2,128)}, u32[]{:S(2)}) copy-start(f32[192,2]{0,1:T(2,128)} %param.31) | copy-start | bytes 4612
  15.2 84.8 %copy-start.17 = (bf16[192,128]{1,0:T(8,128)(2,1)S(1)}, bf16[192,128]{1,0:T(8,128)(2,1)}, u32[]{:S(2)}) copy-start(bf16[192,128]{1,0:T(8,128)(2,1)} %param.28) | copy-start | bytes 147460
  15.3 84.8 %copy-start.18 = (f32[192,1]{0,1:T(1,128)S(1)}, f32[192,1]{0,1:T(1,128)}, u32[]{:S(2)}) copy-start(f32[192,1]{0,1:T(1,128)} %param.32) | copy-start | bytes 2308
  106.5 1.0 copy-start.1
  109.0 7.4 %copy-start.8 = (s32[192,2]{0,1:T(2,128)S(1)}, s32[192,2]{0,1:T(2,128)}, u32[]{:S(2)}) copy-start(s32[192,2]{0,1:T(2,128)} %param.38) | copy-start | bytes 4612
  109.0 17.3 %all-to-all-start = ((bf16[16,192,128]{2,1,0:T(8,128)(2,1)}), bf16[16,192,128]{2,1,0:T(8,128)(2,1)S(1)}, u32[]{:S(2)}, u32[]{:S(2)}) async-start(bf16[16,192,128]{2,1,0:T(8,128)(2,1)} %bitcast.107), calls=%async_computation | async-start | bytes 1572864 | tf_op jit(solution)/shard_map/all_to_all | solution.py:21
  115.7 24.2 %copy-start.7 = (bf16[192,128]{1,0:T(8,128)(2,1)S(1)}, bf16[192,128]{1,0:T(8,128)(2,1)}, u32[]{:S(2)}) copy-start(bf16[192,128]{1,0:T(8,128)(2,1)} %param.35) | copy-start | bytes 147460
  115.7 24.2 %copy-start.12 = (f32[128]{0:T(128)S(1)}, f32[128]{0:T(128)}, u32[]{:S(2)}) copy-start(f32[128]{0:T(128)} %param.36) | copy-start | bytes 1540
  115.7 38.0 %copy-start.9 = (f32[128]{0:T(128)S(1)}, f32[128]{0:T(128)}, u32[]{:S(2)}) copy-start(f32[128]{0:T(128)} %param.37) | copy-start | bytes 1540
  116.4 200.3 %copy-start.4 = (bf16[128,512]{1,0:T(8,128)(2,1)S(1)}, bf16[128,512]{1,0:T(8,128)(2,1)}, u32[]{:S(2)}) copy-start(bf16[128,512]{1,0:T(8,128)(2,1)} %param.43) | copy-start | bytes 393220
  116.6 201.1 %copy-start.5 = (bf16[128,512]{1,0:T(8,128)(2,1)S(1)}, bf16[128,512]{1,0:T(8,128)(2,1)}, u32[]{:S(2)}) copy-start(bf16[128,512]{1,0:T(8,128)(2,1)} %param.44) | copy-start | bytes 393220
  126.4 207.4 %copy-start.2 = (bf16[4,128,512]{2,1,0:T(8,128)(2,1)S(1)}, bf16[4,128,512]{2,1,0:T(8,128)(2,1)}, u32[]{:S(2)}) copy-start(bf16[4,128,512]{2,1,0:T(8,128)(2,1)} %param.40) | copy-start | bytes 1572868
  154.0 181.0 %copy-start.3 = (bf16[4,128,512]{2,1,0:T(8,128)(2,1)S(1)}, bf16[4,128,512]{2,1,0:T(8,128)(2,1)}, u32[]{:S(2)}) copy-start(bf16[4,128,512]{2,1,0:T(8,128)(2,1)} %param.41) | copy-start | bytes 1572868
  154.9 179.0 %all-to-all-start.1 = ((bf16[32,4,5,128]{3,1,2,0:T(4,128)(2,1)}), bf16[32,4,5,128]{3,1,2,0:T(4,128)(2,1)S(1)}, u32[]{:S(2)}, u32[]{:S(2)}) async-start(bf16[32,4,5,128]{3,1,2,0:T(4,128)(2,1)} %copy.143), calls=%async_computation.1 | async-start | bytes 327680 | tf_op jit(solution)/shard_map/all_to_all | solution.py:195
  316.7 125.9 %all-reduce.3.cloned.1.call-start = ((), (), s32[]{:S(2)}) async-start(), calls=%async_computation.4 | async-start | bytes 3407872 | tf_op jit(solution)/shard_map/psum | solution.py:199
  335.0 107.6 %copy-start.13 = (bf16[4,512,128]{2,1,0:T(8,128)(2,1)S(1)}, bf16[4,512,128]{2,1,0:T(8,128)(2,1)}, u32[]{:S(2)}) copy-start(bf16[4,512,128]{2,1,0:T(8,128)(2,1)} %param.42) | copy-start | bytes 1572868
  442.6 17.7 %copy-start.11 = (f32[192,2]{0,1:T(2,128)S(1)}, f32[192,2]{0,1:T(2,128)}, u32[]{:S(2)}) copy-start(f32[192,2]{0,1:T(2,128)} %param.39) | copy-start | bytes 4612
  444.4 35.2 %copy-start.14 = (bf16[192,512]{1,0:T(8,128)(2,1)S(1)}, bf16[192,512]{1,0:T(8,128)(2,1)}, u32[]{:S(2)}) copy-start(bf16[192,512]{1,0:T(8,128)(2,1)} %get-tuple-element.401) | copy-start | bytes 589828
  444.5 35.2 %copy-start.15 = (bf16[192,512]{1,0:T(8,128)(2,1)S(1)}, bf16[192,512]{1,0:T(8,128)(2,1)}, u32[]{:S(2)}) copy-start(bf16[192,512]{1,0:T(8,128)(2,1)} %get-tuple-element.402) | copy-start | bytes 589828
  444.5 35.2 %copy-start.16 = (bf16[512,128]{1,0:T(8,128)(2,1)S(1)}, bf16[512,128]{1,0:T(8,128)(2,1)}, u32[]{:S(2)}) copy-start(bf16[512,128]{1,0:T(8,128)(2,1)} %param.45) | copy-start | bytes 393220
  445.2 31.7 %all-to-all-start.2 = ((bf16[32,4,5,128]{3,1,2,0:T(4,128)(2,1)}), bf16[32,4,5,128]{3,1,2,0:T(4,128)(2,1)S(1)}, u32[]{:S(2)}, u32[]{:S(2)}) async-start(bf16[32,4,5,128]{3,1,2,0:T(4,128)(2,1)} %copy.146), calls=%async_computation.2 | async-start | bytes 327680 | tf_op jit(solution)/shard_map/all_to_all | solution.py:202
Sparse Core Ops, SparseCore 0:
  9.5 81.8 all-gather.1
  336.4 106.1 all-reduce.2
where the time goes:
time: 491 us; the launch traced here: 487 us
  waiting for transfers between devices  224 us (46%)
  starting transfers between devices  183 us (37%)
  blocking collectives  26.9 us (5%)
  local copies, waits for them, and re-layouts  19.3 us (4%)
  matrix products  14.7 us (3%)
  between operations  13.9 us (3%)
    all_to_all x1, starting transfers between devices, shards(): lax.all_to_all(outgoing, 'sp', split_axis=0, concat_axis=0, tiled=True)  162 us
    psum x1, waiting for transfers between devices, shards(): up_pre = lax.psum(up_part.astype(jnp.bfloat16), TP).astype(jnp.float32)  106 us
    all_gather x1, waiting for transfers between devices, shards(): gathered = lax.all_gather(joined_local, 'sp', axis=0, tiled=True)  76.1 us
    psum x4, blocking collectives, by_axis(): x = lax.psum(x, axis)  26.9 us
    all_to_all x1, waiting for transfers between devices, shards(): lax.all_to_all(produced.astype(jnp.bfloat16), 'sp', split_axis=0, concat_...  16.5 us
    all_to_all x1, waiting for transfers between devices, shards(): lax.all_to_all(outgoing, 'sp', split_axis=0, concat_axis=0, tiled=True)  15.2 us
    all_to_all x1, starting transfers between devices, shards(): lax.all_to_all(produced.astype(jnp.bfloat16), 'sp', split_axis=0, concat_...  14.6 us
  transfers between devices with their start and end apart: 5, of which 5 were waited for; matrix products, arithmetic and copies ran while one was open for 2% of the time, Pallas kernels for 0%

commit v1 on v0

v1 whole, which is shorter than its diff:
```python
import functools

import jax
import jax.numpy as jnp
import numpy as np
from jax import lax
from jax.experimental import pallas as pl
from jax.experimental.pallas import tpu as pltpu
from jax.sharding import PartitionSpec as P

D = 2048
EPS = 1e-06
MESH = pl.DeviceIdType.MESH
BF = jnp.bfloat16
F32 = jnp.float32
LANES = 128
CAP = 5
PADDED = 24


def dot(a, b):
    return jnp.dot(a, b, preferred_element_type=F32)


def softplus_block(query, keys, stop, scale, later, valid):
    scores = lax.dot_general(query, keys, (((1,), (1,)), ((), ())), preferred_element_type=F32)
    z = scores * scale + stop
    sp = jnp.maximum(z, 0.0) + jnp.log(1.0 + jnp.exp(-jnp.abs(z)))
    if valid is not None:
        sp = jnp.where(valid, sp, 0.0)
    after = dot(sp.astype(BF), later)
    weight = jnp.exp(z - sp - after)
    if valid is not None:
        weight = jnp.where(valid, weight, 0.0)
    return weight.astype(BF), jnp.sum(sp, axis=1, keepdims=True)


def attention_kernel(
    nz, qa, ka, va, qb, kb, vb, sa, sb, out, buf, accn, accf, ln, later, ssu, rsu, ssd, rsd, ssp, rsp, sloc
):
    rows = qa.shape[0]
    up_steps = nz // 2
    down_steps = nz - 1 - up_steps
    last_far = nz - 2 - up_steps
    sp = lax.axis_index("sp")
    tp = lax.axis_index("tp")
    z = sp // 2
    c = sp % 2
    up_id = (2 * ((z + 1) % nz) + c, tp)
    down_id = (2 * ((z + nz - 1) % nz) + c, tp)
    pair_id = (2 * z + 1 - c, tp)
    barrier = pltpu.get_barrier_semaphore()
    for peer in (up_id, down_id, pair_id):
        pl.semaphore_signal(barrier, inc=1, device_id=peer, device_id_type=MESH)
    pl.semaphore_wait(barrier, 3)

    mine = pl.ds(pl.multiple_of(c * rows, rows), rows)
    srcs = (ka, va, kb, vb)

    def place(block, a):
        return buf.at[block, a, mine, :]

    def other(block, a):
        return buf.at[block, a, pl.ds(pl.multiple_of((1 - c) * rows, rows), rows), :]

    def up_copy(step, a, src):
        block = z + 1 - step
        return pltpu.make_async_remote_copy(
            src_ref=src, dst_ref=place(block, a), send_sem=ssu.at[step - 1, a], recv_sem=rsu.at[step - 1, a],
            device_id=up_id, device_id_type=MESH)

    def down_copy(step, a, src):
        block = (z + step - 1) % nz
        return pltpu.make_async_remote_copy(
            src_ref=src, dst_ref=place(block, a), send_sem=ssd.at[step - 1, a], recv_sem=rsd.at[step - 1, a],
            device_id=down_id, device_id_type=MESH)

    def pair_copy(index, block, a, src):
        return pltpu.make_async_remote_copy(
            src_ref=src, dst_ref=place(block, a), send_sem=ssp.at[index, a], recv_sem=rsp.at[index, a],
            device_id=pair_id, device_id_type=MESH)

    def wait_on(block_ref, sem):
        pltpu.make_async_copy(block_ref, block_ref, sem).wait()

    def sends_up(step):
        return (z < nz - 1) & (z + 1 - step >= 0)

    def sends_down(step):
        return (z + step - 1) % nz <= last_far

    def gets_up(step):
        return z - step >= 0

    def gets_down(step):
        return (z + step) % nz <= last_far

    def far(step):
        return z + step >= nz

    for a in range(4):
        @pl.when(sends_up(1))
        def _(a=a):
            up_copy(1, a, srcs[a]).start()

        @pl.when(sends_down(1))
        def _(a=a):
            down_copy(1, a, srcs[a]).start()

        pair_copy(0, z, a, srcs[a]).start()
        pltpu.make_async_copy(srcs[a], place(z, a), sloc.at[a]).start()

    wide = 2 * rows
    j = lax.broadcasted_iota(jnp.int32, (wide, wide), 0)
    s = lax.broadcasted_iota(jnp.int32, (wide, wide), 1)
    later[...] = (j > s).astype(BF)
    accf[...] = jnp.zeros_like(accf)
    half = lax.broadcasted_iota(jnp.int32, (rows, LANES), 1) < LANES // 2
    qa_all = qa[...]
    zero = jnp.zeros_like(qa_all)
    qa_heads = (jnp.where(half, qa_all, zero), jnp.where(half, zero, qa_all))

    def group_a(block, valid=None):
        keys = buf[block, 0]
        values = buf[block, 1]
        pieces = [
            softplus_block(qa_heads[h], keys, sa[:, h : h + 1], 64 ** -0.5, later[...], valid) for h in range(2)
        ]
        added = jnp.where(half, dot(pieces[0][0], values), dot(pieces[1][0], values))
        return added, jnp.where(half, pieces[0][1], pieces[1][1])

    def group_b(block, valid=None):
        weight, total = softplus_block(qb[...], buf[block, 2], sb[...], 128 ** -0.5, later[...], valid)
        return dot(weight, buf[block, 3]), jnp.broadcast_to(total, (rows, LANES))

    groups = (group_a, group_b)

    def cols(g):
        return slice(g * LANES, (g + 1) * LANES)

    def near(g, step):
        block = z - step
        for a in (2 * g, 2 * g + 1):
            wait_on(other(block, a), rsp.at[step, a])
        added, total = groups[g](block)
        accn[:, cols(g)] += jnp.exp(-ln[:, cols(g)]) * added
        ln[:, cols(g)] += total

    def distant(g, step):
        block = z + step - nz
        for a in (2 * g, 2 * g + 1):
            wait_on(other(block, a), rsp.at[up_steps + step, a])
        added, total = groups[g](block)
        accf[:, cols(g)] = jnp.exp(-total) * accf[:, cols(g)] + added

    def poll_up(step, a):
        @pl.when(gets_up(step))
        def _():
            ref = place(z - step, a)
            wait_on(ref, rsu.at[step - 1, a])

            @pl.when((step < up_steps) & (z < nz - 1))
            def _():
                up_copy(step + 1, a, ref).start()

            pair_copy(step, z - step, a, ref).start()

    def poll_down(step, a):
        @pl.when((step <= down_steps) & gets_down(step))
        def _():
            block = (z + step) % nz
            ref = place(block, a)
            wait_on(ref, rsd.at[step - 1, a])

            @pl.when(step < down_steps)
            def _():
                down_copy(step + 1, a, ref).start()

            @pl.when(far(step))
            def _():
                pair_copy(up_steps + step, block, a, ref).start()

    row_at = lax.broadcasted_iota(jnp.int32, (rows, wide), 0) + c * rows
    key_at = lax.broadcasted_iota(jnp.int32, (rows, wide), 1)
    valid = key_at < row_at
    for g in range(2):
        for a in (2 * g, 2 * g + 1):
            wait_on(place(z, a), sloc.at[a])
            wait_on(other(z, a), rsp.at[0, a])
        added, total = groups[g](z, valid)
        accn[:, cols(g)] = added
        ln[:, cols(g)] = total
        for a in (2 * g, 2 * g + 1):
            poll_up(1, a)
            poll_down(1, a)

    @pl.loop(2, up_steps + 1)
    def _(step):
        before = step - 1
        for a in range(4):
            poll_up(step, a)
            poll_down(step, a)
            g = a // 2
            if a % 2 == 0:
                @pl.when(gets_up(before))
                def _():
                    near(g, before)
            else:
                @pl.when(far(before))
                def _():
                    distant(g, before)

    @pl.when(gets_up(up_steps))
    def _():
        for g in range(2):
            near(g, up_steps)

    out[...] = (accn[...] + jnp.exp(-ln[...]) * accf[...]).astype(BF)

    for a in range(4):
        pair_copy(0, z, a, srcs[a]).wait_send()

    @pl.loop(1, up_steps + 1)
    def _(step):
        for a in range(4):
            @pl.when(sends_up(step))
            def _():
                up_copy(step, a, place(z + 1 - step, a)).wait_send()

            @pl.when(gets_up(step))
            def _():
                pair_copy(step, z - step, a, place(z - step, a)).wait_send()

    @pl.loop(1, down_steps + 1)
    def _(step):
        for a in range(4):
            @pl.when(sends_down(step))
            def _():
                down_copy(step, a, place((z + step - 1) % nz, a)).wait_send()

            @pl.when(far(step))
            def _():
                pair_copy(up_steps + step, z + step - nz, a, place(z + step - nz, a)).wait_send()


def attention(nz, *arrays):
    rows = arrays[0].shape[0]
    up_steps = nz // 2
    down_steps = nz - 1 - up_steps
    dma = pltpu.SemaphoreType.DMA
    return pl.pallas_call(
        functools.partial(attention_kernel, nz),
        out_shape=jax.ShapeDtypeStruct((rows, 2 * LANES), BF),
        in_specs=[pl.BlockSpec(memory_space=pltpu.VMEM)] * 8,
        out_specs=pl.BlockSpec(memory_space=pltpu.VMEM),
        scratch_shapes=[
            pltpu.VMEM((nz, 4, 2 * rows, LANES), BF),
            pltpu.VMEM((rows, 2 * LANES), F32),
            pltpu.VMEM((rows, 2 * LANES), F32),
            pltpu.VMEM((rows, 2 * LANES), F32),
            pltpu.VMEM((2 * rows, 2 * rows), BF),
            dma((up_steps, 4)),
            dma((up_steps, 4)),
            dma((down_steps, 4)),
            dma((down_steps, 4)),
            dma((nz, 4)),
            dma((nz, 4)),
            dma((4,)),
        ],
        compiler_params=pltpu.CompilerParams(
            collective_id=0, has_side_effects=True, vmem_limit_bytes=48 * 1024 * 1024),
    )(*arrays)


TP = ("tp",)


def sum_at_owner(x, axis, dim):
    n = lax.axis_size(axis)
    tiles = jnp.moveaxis(x.reshape(x.shape[0], n, -1), 1, 0)
    arrived = lax.all_to_all(tiles, axis, split_axis=0, concat_axis=0, tiled=True)
    return arrived.astype(F32).sum(axis=0)


def rest(attended, out_a, out_b, resid, mix_gain, ffn_gain, routes, gates, exp_gate, exp_up, exp_down, sh_gate, sh_up, sh_down):
    rows = resid.shape[0]
    n_sp = lax.axis_size("sp")
    part = dot(attended[:, :LANES], out_a) + dot(attended[:, LANES:], out_b)
    mixed = sum_at_owner(part.astype(BF), "tp", 1)
    mix_total = lax.psum(jnp.sum(mixed * mixed, axis=1), "tp")
    branch = mixed * lax.rsqrt(mix_total / D + EPS)[:, None] * mix_gain[None, :]
    stream = lax.optimization_barrier((resid.astype(F32) + branch).astype(BF))
    stream_f = stream.astype(F32)
    ffn_total = lax.psum(jnp.sum(stream_f * stream_f, axis=1), "tp")
    normed = (stream_f * lax.rsqrt(ffn_total / D + EPS)[:, None] * ffn_gain[None, :]).astype(BF)
    shared_gate = lax.psum(dot(normed, sh_gate).astype(BF), "tp").astype(F32)
    shared_up = lax.psum(dot(normed, sh_up).astype(BF), "tp").astype(F32)
    shared_hidden = (jax.nn.silu(shared_gate) * shared_up).astype(BF)
    shared_out = dot(shared_hidden, sh_down)
    local_experts = exp_gate.shape[0]
    experts = local_experts * n_sp
    top_count = routes.shape[1]
    capacity = CAP
    flat_routes = routes.reshape(-1)
    onehot = (flat_routes[:, None] == jnp.arange(experts, dtype=jnp.int32)[None, :]).astype(jnp.int32)
    earlier = jnp.cumsum(onehot, axis=0) - onehot
    slot = flat_routes * capacity + jnp.sum(earlier * onehot, axis=1)
    chooser = (slot[:, None] == jnp.arange(experts * capacity, dtype=jnp.int32)[None, :]).astype(BF)
    chooser = jnp.sum(chooser.reshape(rows, top_count, experts * capacity), axis=1)
    outgoing = jnp.einsum("rs,rc->sc", chooser, normed, preferred_element_type=F32).astype(BF)
    outgoing = outgoing.reshape(n_sp, local_experts, capacity, normed.shape[1])
    arrived = lax.all_to_all(outgoing, "sp", split_axis=0, concat_axis=0, tiled=True)
    gate_part = jnp.einsum("segd,edf->segf", arrived, exp_gate, preferred_element_type=F32)
    up_part = jnp.einsum("segd,edf->segf", arrived, exp_up, preferred_element_type=F32)
    gate_pre = lax.psum(gate_part.astype(BF), "tp").astype(F32)
    up_pre = lax.psum(up_part.astype(BF), "tp").astype(F32)
    hidden = (jax.nn.silu(gate_pre) * up_pre).astype(BF)
    produced = jnp.einsum("segf,efd->segd", hidden, exp_down, preferred_element_type=F32)
    returned = lax.all_to_all(produced.astype(BF), "sp", split_axis=0, concat_axis=0, tiled=True)
    flat_back = returned.reshape(experts * capacity, returned.shape[3])
    picked = jnp.take(flat_back, slot, axis=0).reshape(rows, top_count, returned.shape[3])
    routed = jnp.sum(gates[:, :, None] * picked.astype(F32), axis=1)
    return (stream_f + (routed + shared_out)).astype(BF)


def shards(query_a, key_a, value_a, query_b, key_b, value_b, stop_a, stop_b, *others):
    nz = lax.axis_size("sp") // 2
    attended = attention(nz, query_a, key_a, value_a, query_b, key_b, value_b, stop_a, stop_b)
    return rest(attended, *others)


def solution(mesh):
    row, col, both = P("tp", None), P("tp"), P("sp", "tp")
    in_specs = (both,) * 8 + (
        row, row, both, col, col, P("sp", None), P("sp", None),
        P("sp", "tp", None), P("sp", "tp", None), P("sp", None, "tp"), row, row, P(None, "tp"))
    return jax.shard_map(shards, mesh=mesh, in_specs=in_specs, out_specs=both, check_vma=False)
```

time: 491 us -> 342 us (0.70)
  starting transfers between devices: 183 us -> 55.2 us
  waiting for transfers between devices: 224 us -> 149 us
  Pallas kernels: 0 us -> 42 us
  blocking collectives: 26.9 us -> 59 us
  local copies, waits for them, and re-layouts: 19.3 us -> 12 us
  matrix products: 14.7 us -> 7.99 us
    all_to_all x2, starting transfers between devices: 176 us -> 48.4 us  [the longest x1 33.7 us: rest(): lax.all_to_all(outgoing, 'sp', split_axis=0, concat_axis=0, tiled=True)]
    all_gather x1 -> x0, waiting for transfers between devices: 76.1 us -> none  [shards(): gathered = lax.all_gather(joined_local, 'sp', axis=0, tiled=True)]
    pallas_call x0 -> x1, Pallas kernels: none -> 42 us  [attention(): pl.pallas_call(functools.partial(attention_kernel, nz), out_shape=jax.Sha...]
    psum x4 -> x2, blocking collectives: 26.9 us -> 59 us  [the longest x1 29.5 us: rest(): mix_total = lax.psum(jnp.sum(mixed * mixed, axis=1), 'tp')]
    while x1 -> x0, local copies, waits for them, and re-layouts: 8.7 us -> none  [shards(): state = lax.fori_loop(1, n_sp, turn, state)]
    dot_general x17 -> x9, matrix products: 14.7 us -> 7.99 us  [the longest x5 3.46 us: dot(): return jnp.dot(a, b, preferred_element_type=F32)]
  transfers between devices with their start and end apart: 5 -> 4, of which waited for: 5 -> 4; matrix products, arithmetic and copies ran while one was open for 2% -> 1% of each run, Pallas kernels for 0% -> 0%
where the time goes in v1:
time: 342 us; the launch traced here: 341 us
  waiting for transfers between devices  149 us (44%)
  blocking collectives  59 us (17%)
  starting transfers between devices  55.2 us (16%)
  Pallas kernels  42 us (12%)
  between operations  13.8 us (4%)
  local copies, waits for them, and re-layouts  12 us (4%)
  matrix products  7.99 us (2%)
    psum x1, waiting for transfers between devices, rest(): up_pre = lax.psum(up_part.astype(BF), 'tp').astype(F32)  106 us
    pallas_call x1, Pallas kernels, attention(): pl.pallas_call(functools.partial(attention_kernel, nz), out_shape=jax.Sha...  42 us
    all_to_all x1, starting transfers between devices, rest(): lax.all_to_all(outgoing, 'sp', split_axis=0, concat_axis=0, tiled=True)  33.7 us
    psum x1, blocking collectives, rest(): mix_total = lax.psum(jnp.sum(mixed * mixed, axis=1), 'tp')  29.5 us
    psum x1, blocking collectives, rest(): ffn_total = lax.psum(jnp.sum(stream_f * stream_f, axis=1), 'tp')  29.4 us
    all_to_all x1, waiting for transfers between devices, rest(): lax.all_to_all(produced.astype(BF), 'sp', split_axis=0, concat_axis=0, ti...  16.5 us
    all_to_all x1, waiting for transfers between devices, rest(): lax.all_to_all(outgoing, 'sp', split_axis=0, concat_axis=0, tiled=True)  15.2 us
    all_to_all x1, starting transfers between devices, rest(): lax.all_to_all(produced.astype(BF), 'sp', split_axis=0, concat_axis=0, ti...  14.7 us
  transfers between devices with their start and end apart: 4, of which 4 were waited for; matrix products, arithmetic and copies ran while one was open for 1% of the time, Pallas kernels for 0%

profile of v1, /device:TPU:1, one launch (start us, length us, event | category | flops | bytes accessed | tf_op | source)
XLA Modules:
  0.0 341.3 jit_solution(11329938066275372666)
XLA Ops:
  6.5 0.0 copy-start
  6.5 0.8 copy.79.sa
  7.4 0.8 copy.80.sb
  8.2 0.0 copy-start.1
  8.2 0.8 copy-done.1
  9.0 0.8 copy-done.2
  9.8 0.8 copy-done.3
  10.6 0.8 copy-done.4
  11.4 0.8 copy-done.5
  12.2 0.8 copy-done.6
  13.0 42.0 %shard_map.199 = bf16[192,256]{1,0:T(8,128)(2,1)S(1)} custom-call(bf16[192,128]{1,0:T(8,128)(2,1)S(1)} %copy-done.1, bf16[192,128]{1,0:T(8,128)(2,1)S(1)} %copy-done.2, bf16[192,128]{1,0:T(8,128)(2,1)S(1)} %copy-done.3, bf16[192,128]{1,0:T(8,128)(2,1)S(1)} %copy-done.4, bf16[192,128]{1,0:T(8,128)(2,1)S(1)} %copy-done.5, bf16[192,128]{1,0:T(8,128)(2,1)S(1)} %copy-done.6, ...), custom_call_target="tpu_custom_call" | custom-call | tf_op jit(solution)/shard_map/pallas_call | solution.py:251
  55.0 0.4 fusion.35
  55.4 0.4 fusion.6
  55.8 0.0 copy-start.13
  55.8 1.1 copy.104
  56.8 6.7 %all-to-all-start = ((bf16[16,192,128]{2,1,0:T(8,128)(2,1)}), bf16[16,192,128]{2,1,0:T(8,128)(2,1)S(1)}, u32[]{:S(2)}, u32[]{:S(2)}) async-start(bf16[16,192,128]{2,1,0:T(8,128)(2,1)} %bitcast.45), calls=%async_computation | async-start | bytes 1572864 | tf_op jit(solution)/shard_map/all_to_all | solution.py:281
  63.6 0.1 copy.83
  63.7 0.1 eq.40
  63.9 0.1 copy.85
  64.0 0.2 fusion.23
  64.2 0.1 reshape.91
  64.4 0.0 copy-start.14
  64.5 0.2 fusion.26
  64.7 0.1 reduce_sum.64
  64.9 0.1 copy.87
  65.0 0.2 fusion.17
  65.1 0.0 copy-start.10
  65.2 11.1 %all-to-all-done = bf16[16,192,128]{2,1,0:T(8,128)(2,1)S(1)} async-done(((bf16[16,192,128]{2,1,0:T(8,128)(2,1)}), bf16[16,192,128]{2,1,0:T(8,128)(2,1)S(1)}, u32[]{:S(2)}, u32[]{:S(2)}) %all-to-all-start) | async-done | bytes 786464 | tf_op jit(solution)/shard_map/all_to_all | solution.py:281
  76.3 0.1 convert_reduce_fusion
  76.4 0.0 copy-start.11
  76.4 0.1 multiply_reduce_fusion.1
  76.5 29.5 %psum.42 = f32[192]{0:T(256)S(1)} all-reduce(f32[192]{0:T(256)S(1)} %multiply_reduce_fusion.1), channel_id=1, replica_groups=mesh['sp'=32,'tp'=16] {'tp'}, use_global_device_ids=true, to_apply=%region_2.0 | all-reduce | flops 192 | bytes 1536 | tf_op jit(solution)/shard_map/psum | solution.py:290
  106.1 0.0 copy-done.12
  106.1 0.0 copy-start.8
  106.1 0.1 add_convert_fusion
  106.2 0.1 fusion.31
  106.3 29.4 %psum.43 = f32[192]{0:T(256)S(1)} all-reduce(f32[192]{0:T(256)S(1)} %fusion.31), channel_id=1, replica_groups=mesh['sp'=32,'tp'=16] {'tp'}, use_global_device_ids=true, to_apply=%region_8.9 | all-reduce | flops 192 | bytes 1536 | tf_op jit(solution)/shard_map/psum | solution.py:294
  135.8 0.3 convolution_convert_fusion.5
  136.1 0.1 reshape.93
  136.2 0.7 copy.89
  136.9 33.7 %all-to-all-start.1 = ((bf16[32,4,5,128]{3,1,2,0:T(4,128)(2,1)}), bf16[32,4,5,128]{3,1,2,0:T(4,128)(2,1)S(1)}, u32[]{:S(2)}, u32[]{:S(2)}) async-start(bf16[32,4,5,128]{3,1,2,0:T(4,128)(2,1)} %copy.89), calls=%async_computation.1 | async-start | bytes 327680 | tf_op jit(solution)/shard_map/all_to_all | solution.py:312
  170.6 0.0 all-reduce.3.cloned.1.call-start
  170.7 0.9 convolution_convert_fusion.3
  171.6 0.0 copy-done.11
  171.6 0.9 convolution_convert_fusion.2
  172.5 15.2 %all-to-all-done.1 = bf16[32,4,5,128]{3,1,2,0:T(4,128)(2,1)S(1)} async-done(((bf16[32,4,5,128]{3,1,2,0:T(4,128)(2,1)}), bf16[32,4,5,128]{3,1,2,0:T(4,128)(2,1)S(1)}, u32[]{:S(2)}, u32[]{:S(2)}) %all-to-all-start.1) | async-done | bytes 163872 | tf_op jit(solution)/shard_map/all_to_all | solution.py:312
  187.7 0.0 copy-done.8
  187.7 1.2 fusion.7
  188.9 1.2 fusion.8
  190.1 0.0 all-reduce.3.cloned.1.call-update
  190.1 106.2 %all-reduce.3.cloned.1.call-done = (bf16[32,4,5,512]{3,0,2,1:T(8,128)(2,1)}, bf16[32,4,5,512]{3,0,2,1:T(8,128)(2,1)}, bf16[192,512]{1,0:T(8,128)(2,1)}, bf16[192,512]{1,0:T(8,128)(2,1)}) async-done(((bf16[32,4,5,512]{3,0,2,1:T(8,128)(2,1)}, bf16[32,4,5,512]{3,0,2,1:T(8,128)(2,1)}, bf16[192,512]{1,0:T(8,128)(2,1)}, bf16[192,512]{1,0:T(8,128)(2,1)}), (bf16[32,4,5,512]{3,0,2,1:T(8,128)(2,1)}, ...) | async-done | bytes 1703952 | tf_op jit(solution)/shard_map/psum | solution.py:316
  296.3 1.8 fusion.9
  298.2 0.7 copy.92
  298.9 14.7 %all-to-all-start.2 = ((bf16[32,4,5,128]{3,1,2,0:T(4,128)(2,1)}), bf16[32,4,5,128]{3,1,2,0:T(4,128)(2,1)S(1)}, u32[]{:S(2)}, u32[]{:S(2)}) async-start(bf16[32,4,5,128]{3,1,2,0:T(4,128)(2,1)} %copy.92), calls=%async_computation.2 | async-start | bytes 327680 | tf_op jit(solution)/shard_map/all_to_all | solution.py:319
  313.7 0.1 copy.94
  313.8 0.1 mul.101
  314.0 0.2 copy.88
  314.2 0.1 copy.82
  314.3 16.5 %all-to-all-done.2 = bf16[32,4,5,128]{3,1,2,0:T(4,128)(2,1)S(1)} async-done(((bf16[32,4,5,128]{3,1,2,0:T(4,128)(2,1)}), bf16[32,4,5,128]{3,1,2,0:T(4,128)(2,1)S(1)}, u32[]{:S(2)}, u32[]{:S(2)}) %all-to-all-start.2) | async-done | bytes 163872 | tf_op jit(solution)/shard_map/all_to_all | solution.py:319
  330.8 0.1 copy.93
  330.9 0.1 reshape.94
  331.0 1.4 gather_fusion
  332.4 1.1 multiply_reduce_fusion
  333.6 0.9 fusion.11
  (36 shorter events, 0.2 us)
Async XLA Ops:
  6.5 48.5 %copy-start = (bf16[128,2048]{1,0:T(8,128)(2,1)S(1)}, bf16[128,2048]{1,0:T(8,128)(2,1)}, u32[]{:S(2)}) copy-start(bf16[128,2048]{1,0:T(8,128)(2,1)} %param.29) | copy-start | bytes 1572868
  8.2 0.8 copy-start.1
  9.0 0.8 copy-start.2
  9.8 0.8 copy-start.3
  10.6 0.8 copy-start.4
  11.4 0.8 copy-start.5
  12.2 0.8 copy-start.6
  13.0 42.4 %copy-start.7 = (bf16[128,2048]{1,0:T(8,128)(2,1)S(1)}, bf16[128,2048]{1,0:T(8,128)(2,1)}, u32[]{:S(2)}) copy-start(bf16[128,2048]{1,0:T(8,128)(2,1)} %param.30) | copy-start | bytes 1572868
  55.8 7.9 %copy-start.13 = (s32[192,2]{0,1:T(2,128)S(1)}, s32[192,2]{0,1:T(2,128)}, u32[]{:S(2)}) copy-start(s32[192,2]{0,1:T(2,128)} %param.34) | copy-start | bytes 4612
  56.8 19.4 %all-to-all-start = ((bf16[16,192,128]{2,1,0:T(8,128)(2,1)}), bf16[16,192,128]{2,1,0:T(8,128)(2,1)S(1)}, u32[]{:S(2)}, u32[]{:S(2)}) async-start(bf16[16,192,128]{2,1,0:T(8,128)(2,1)} %bitcast.45), calls=%async_computation | async-start | bytes 1572864 | tf_op jit(solution)/shard_map/all_to_all | solution.py:281
  64.4 41.7 %copy-start.12 = (bf16[192,128]{1,0:T(8,128)(2,1)S(1)}, bf16[192,128]{1,0:T(8,128)(2,1)}, u32[]{:S(2)}) copy-start(bf16[192,128]{1,0:T(8,128)(2,1)} %param.31) | copy-start | bytes 147460
  64.4 41.7 %copy-start.16 = (f32[128]{0:T(128)S(1)}, f32[128]{0:T(128)}, u32[]{:S(2)}) copy-start(f32[128]{0:T(128)} %param.32) | copy-start | bytes 1540
  64.4 71.4 %copy-start.14 = (f32[128]{0:T(128)S(1)}, f32[128]{0:T(128)}, u32[]{:S(2)}) copy-start(f32[128]{0:T(128)} %param.33) | copy-start | bytes 1540
  65.1 105.5 %copy-start.10 = (bf16[128,512]{1,0:T(8,128)(2,1)S(1)}, bf16[128,512]{1,0:T(8,128)(2,1)}, u32[]{:S(2)}) copy-start(bf16[128,512]{1,0:T(8,128)(2,1)} %param.39) | copy-start | bytes 393220
  76.4 95.2 %copy-start.11 = (bf16[128,512]{1,0:T(8,128)(2,1)S(1)}, bf16[128,512]{1,0:T(8,128)(2,1)}, u32[]{:S(2)}) copy-start(bf16[128,512]{1,0:T(8,128)(2,1)} %param.40) | copy-start | bytes 393220
  106.1 81.7 %copy-start.8 = (bf16[4,128,512]{2,1,0:T(8,128)(2,1)S(1)}, bf16[4,128,512]{2,1,0:T(8,128)(2,1)}, u32[]{:S(2)}) copy-start(bf16[4,128,512]{2,1,0:T(8,128)(2,1)} %param.36) | copy-start | bytes 1572868
  136.9 52.0 %copy-start.9 = (bf16[4,128,512]{2,1,0:T(8,128)(2,1)S(1)}, bf16[4,128,512]{2,1,0:T(8,128)(2,1)}, u32[]{:S(2)}) copy-start(bf16[4,128,512]{2,1,0:T(8,128)(2,1)} %param.37) | copy-start | bytes 1572868
  136.9 50.8 %all-to-all-start.1 = ((bf16[32,4,5,128]{3,1,2,0:T(4,128)(2,1)}), bf16[32,4,5,128]{3,1,2,0:T(4,128)(2,1)S(1)}, u32[]{:S(2)}, u32[]{:S(2)}) async-start(bf16[32,4,5,128]{3,1,2,0:T(4,128)(2,1)} %copy.89), calls=%async_computation.1 | async-start | bytes 327680 | tf_op jit(solution)/shard_map/all_to_all | solution.py:312
  170.6 125.7 %all-reduce.3.cloned.1.call-start = ((), (), s32[]{:S(2)}) async-start(), calls=%async_computation.3 | async-start | bytes 3407872 | tf_op jit(solution)/shard_map/psum | solution.py:316
  188.9 107.4 %copy-start.17 = (bf16[4,512,128]{2,1,0:T(8,128)(2,1)S(1)}, bf16[4,512,128]{2,1,0:T(8,128)(2,1)}, u32[]{:S(2)}) copy-start(bf16[4,512,128]{2,1,0:T(8,128)(2,1)} %param.38) | copy-start | bytes 1572868
  296.3 17.8 %copy-start.15 = (f32[192,2]{0,1:T(2,128)S(1)}, f32[192,2]{0,1:T(2,128)}, u32[]{:S(2)}) copy-start(f32[192,2]{0,1:T(2,128)} %param.35) | copy-start | bytes 4612
  298.9 34.6 %copy-start.18 = (bf16[192,512]{1,0:T(8,128)(2,1)S(1)}, bf16[192,512]{1,0:T(8,128)(2,1)}, u32[]{:S(2)}) copy-start(bf16[192,512]{1,0:T(8,128)(2,1)} %get-tuple-element.7) | copy-start | bytes 589828
  298.9 34.6 %copy-start.19 = (bf16[192,512]{1,0:T(8,128)(2,1)S(1)}, bf16[192,512]{1,0:T(8,128)(2,1)}, u32[]{:S(2)}) copy-start(bf16[192,512]{1,0:T(8,128)(2,1)} %get-tuple-element.8) | copy-start | bytes 589828
  298.9 34.6 %copy-start.20 = (bf16[512,128]{1,0:T(8,128)(2,1)S(1)}, bf16[512,128]{1,0:T(8,128)(2,1)}, u32[]{:S(2)}) copy-start(bf16[512,128]{1,0:T(8,128)(2,1)} %param.41) | copy-start | bytes 393220
  298.9 31.9 %all-to-all-start.2 = ((bf16[32,4,5,128]{3,1,2,0:T(4,128)(2,1)}), bf16[32,4,5,128]{3,1,2,0:T(4,128)(2,1)S(1)}, u32[]{:S(2)}, u32[]{:S(2)}) async-start(bf16[32,4,5,128]{3,1,2,0:T(4,128)(2,1)} %copy.92), calls=%async_computation.2 | async-start | bytes 327680 | tf_op jit(solution)/shard_map/all_to_all | solution.py:319
Sparse Core Ops, SparseCore 0:
  190.2 106.0 all-reduce.2

commit v2 on v1

--- a/solution.py
+++ b/solution.py
@@ -272,55 +272,311 @@
     )(*arrays)
 
 
-TP = ("tp",)
-
-
-def sum_at_owner(x, axis, dim):
-    n = lax.axis_size(axis)
-    tiles = jnp.moveaxis(x.reshape(x.shape[0], n, -1), 1, 0)
-    arrived = lax.all_to_all(tiles, axis, split_axis=0, concat_axis=0, tiled=True)
-    return arrived.astype(F32).sum(axis=0)
-
-
-def rest(attended, out_a, out_b, resid, mix_gain, ffn_gain, routes, gates, exp_gate, exp_up, exp_down, sh_gate, sh_up, sh_down):
+def rest_kernel(
+    n_sp, n_tp, att, oa, ob, resid, mg, fg, routes, gates, eg, eu, ed, sg, su, sd, tcol, rcol, out,
+    part, rs, sts, st, dsp_out, dsp_in, ret_out, ret_in, shp, shr, shs, shh, xbuf, gp, gin, hs, hin, obuf, oh, smat, rmat,
+    tp_send, tp_recv, sp_send, sp_recv
+):
     rows = resid.shape[0]
-    n_sp = lax.axis_size("sp")
-    part = dot(attended[:, :LANES], out_a) + dot(attended[:, LANES:], out_b)
-    mixed = sum_at_owner(part.astype(BF), "tp", 1)
-    mix_total = lax.psum(jnp.sum(mixed * mixed, axis=1), "tp")
-    branch = mixed * lax.rsqrt(mix_total / D + EPS)[:, None] * mix_gain[None, :]
-    stream = lax.optimization_barrier((resid.astype(F32) + branch).astype(BF))
-    stream_f = stream.astype(F32)
-    ffn_total = lax.psum(jnp.sum(stream_f * stream_f, axis=1), "tp")
-    normed = (stream_f * lax.rsqrt(ffn_total / D + EPS)[:, None] * ffn_gain[None, :]).astype(BF)
-    shared_gate = lax.psum(dot(normed, sh_gate).astype(BF), "tp").astype(F32)
-    shared_up = lax.psum(dot(normed, sh_up).astype(BF), "tp").astype(F32)
-    shared_hidden = (jax.nn.silu(shared_gate) * shared_up).astype(BF)
-    shared_out = dot(shared_hidden, sh_down)
-    local_experts = exp_gate.shape[0]
-    experts = local_experts * n_sp
-    top_count = routes.shape[1]
-    capacity = CAP
-    flat_routes = routes.reshape(-1)
-    onehot = (flat_routes[:, None] == jnp.arange(experts, dtype=jnp.int32)[None, :]).astype(jnp.int32)
-    earlier = jnp.cumsum(onehot, axis=0) - onehot
-    slot = flat_routes * capacity + jnp.sum(earlier * onehot, axis=1)
-    chooser = (slot[:, None] == jnp.arange(experts * capacity, dtype=jnp.int32)[None, :]).astype(BF)
-    chooser = jnp.sum(chooser.reshape(rows, top_count, experts * capacity), axis=1)
-    outgoing = jnp.einsum("rs,rc->sc", chooser, normed, preferred_element_type=F32).astype(BF)
-    outgoing = outgoing.reshape(n_sp, local_experts, capacity, normed.shape[1])
-    arrived = lax.all_to_all(outgoing, "sp", split_axis=0, concat_axis=0, tiled=True)
-    gate_part = jnp.einsum("segd,edf->segf", arrived, exp_gate, preferred_element_type=F32)
-    up_part = jnp.einsum("segd,edf->segf", arrived, exp_up, preferred_element_type=F32)
-    gate_pre = lax.psum(gate_part.astype(BF), "tp").astype(F32)
-    up_pre = lax.psum(up_part.astype(BF), "tp").astype(F32)
-    hidden = (jax.nn.silu(gate_pre) * up_pre).astype(BF)
-    produced = jnp.einsum("segf,efd->segd", hidden, exp_down, preferred_element_type=F32)
-    returned = lax.all_to_all(produced.astype(BF), "sp", split_axis=0, concat_axis=0, tiled=True)
-    flat_back = returned.reshape(experts * capacity, returned.shape[3])
-    picked = jnp.take(flat_back, slot, axis=0).reshape(rows, top_count, returned.shape[3])
-    routed = jnp.sum(gates[:, :, None] * picked.astype(F32), axis=1)
-    return (stream_f + (routed + shared_out)).astype(BF)
+    units = eg.shape[2]
+    local = eg.shape[0]
+    share = hs.shape[0]
+    quarters = n_tp // local
+    seats = n_sp * PADDED
+    strips = rows // 16
+    sp = lax.axis_index("sp")
+    tp = lax.axis_index("tp")
+    barrier = pltpu.get_barrier_semaphore()
+
+    @pl.loop(1, n_tp)
+    def _(k):
+        pl.semaphore_signal(barrier, inc=1, device_id=(sp, (tp + k) % n_tp), device_id_type=MESH)
+
+    @pl.loop(1, n_sp)
+    def _(k):
+        pl.semaphore_signal(barrier, inc=1, device_id=((sp + k) % n_sp, tp), device_id_type=MESH)
+
+    pl.semaphore_wait(barrier, n_tp + n_sp - 2)
+
+    def tp_copy(phase, g, src, dst):
+        return pltpu.make_async_remote_copy(
+            src_ref=src, dst_ref=dst, send_sem=tp_send.at[phase, g], recv_sem=tp_recv.at[phase, tp],
+            device_id=(sp, g), device_id_type=MESH)
+
+    def sp_copy(phase, d, src, dst):
+        return pltpu.make_async_remote_copy(
+            src_ref=src, dst_ref=dst, send_sem=sp_send.at[phase, d], recv_sem=sp_recv.at[phase, sp],
+            device_id=(d, tp), device_id_type=MESH)
+
+    def landed(ref, sem):
+        pltpu.make_async_copy(ref, ref, sem).wait()
+
+    def after_tp(k):
+        return (tp + k) % n_tp
+
+    def before_tp(k):
+        return (tp + n_tp - k) % n_tp
+
+    low, high = att[:, :LANES], att[:, LANES:]
+
+    @pl.loop(1, n_tp + 1)
+    def _(k):
+        g = after_tp(k)
+        cols = pl.ds(pl.multiple_of(g * LANES, LANES), LANES)
+        part[g] = (dot(low, oa[:, cols]) + dot(high, ob[:, cols])).astype(BF)
+
+        @pl.when(k < n_tp)
+        def _():
+            tp_copy(0, g, part.at[g], rs.at[tp]).start()
+
+    experts = local * n_sp
+    e_at = lax.broadcasted_iota(jnp.int32, (rows, experts), 1)
+    named = [e_at == routes[:, k : k + 1] for k in range(2)]
+    members = jnp.where(named[0] | named[1], 1.0, 0.0).astype(BF)
+    r_at = lax.broadcasted_iota(jnp.int32, (rows, rows), 0)
+    c_at = lax.broadcasted_iota(jnp.int32, (rows, rows), 1)
+    prior = dot((c_at < r_at).astype(BF), members)
+    seat_at = lax.broadcasted_iota(jnp.int32, (rows, seats), 1).astype(F32)
+    wide = 2 * LANES
+    line_at = lax.broadcasted_iota(jnp.int32, (seats, wide), 0).astype(F32)
+    chooser = None
+    for k in range(2):
+        e = routes[:, k : k + 1]
+        rank = jnp.sum(jnp.where(named[k], prior, 0.0), axis=1, keepdims=True)
+        seat = ((e // local) * PADDED + (e % local) * CAP).astype(F32) + rank
+        oh[k] = (seat_at == seat).astype(BF)
+        tall = jnp.concatenate(
+            [jnp.broadcast_to(seat, (rows, LANES)), jnp.full((wide - rows, LANES), -1.0, F32)], axis=0)
+        line = jnp.transpose(tall)[0:1, :]
+        hit = line_at == line
+        chooser = hit if chooser is None else chooser | hit
+    chooser = chooser.astype(BF)
+    lane_at = lax.broadcasted_iota(jnp.int32, (local * n_sp * CAP, seats), 1)
+    smat[...] = (lane_at == tcol[...]).astype(BF)
+    lane_at = lax.broadcasted_iota(jnp.int32, (seats, local * n_sp * CAP), 1)
+    rmat[...] = (lane_at == rcol[...]).astype(BF)
+
+    def gather_rs(k, total):
+        src = before_tp(k)
+        landed(rs.at[src], tp_recv.at[0, src])
+        return total + rs[src].astype(F32)
+
+    mixed = lax.fori_loop(1, n_tp, gather_rs, part[tp].astype(F32))
+
+    def row_total(which, values):
+        own = jnp.broadcast_to(jnp.sum(values, axis=1, keepdims=True), (rows, LANES))
+        tall = jnp.concatenate([own, jnp.zeros((wide - rows, LANES), F32)], axis=0)
+        lines = jnp.transpose(tall)[0:8, :]
+        sts[which] = lines
+
+        @pl.loop(1, n_tp)
+        def _(k):
+            g = after_tp(k)
+            tp_copy(1 + which, g, sts.at[which], st.at[which, tp]).start()
+
+        def gather(k, total):
+            src = before_tp(k)
+            landed(st.at[which, src], tp_recv.at[1 + which, src])
+            return total + st[which, src]
+
+        total = lax.fori_loop(1, n_tp, gather, lines)
+        return jnp.transpose(jnp.broadcast_to(total[0:1, :], (LANES, wide)))[:rows, :]
+
+    scale = lax.rsqrt(row_total(0, mixed * mixed) / D + EPS)
+    stream = (resid[...].astype(F32) + mixed * scale * mg[...]).astype(BF).astype(F32)
+    scale = lax.rsqrt(row_total(1, stream * stream) / D + EPS)
+    normed = (stream * scale * fg[...]).astype(BF)
+
+    tall = jnp.concatenate([normed, jnp.zeros((wide - rows, LANES), BF)], axis=0)
+    dsp_out[...] = dot(chooser, tall).reshape(n_sp, PADDED, LANES).astype(BF)
+
+    @pl.loop(1, n_sp)
+    def _(k):
+        d = (sp + k) % n_sp
+        sp_copy(0, d, dsp_out.at[d], dsp_in.at[sp]).start()
+
+    dsp_in[sp] = dsp_out[sp]
+
+    shp[:, :, :units] = dot(normed, sg[...]).reshape(strips, 16, units).astype(BF)
+    shp[:, :, units:] = dot(normed, su[...]).reshape(strips, 16, units).astype(BF)
+
+    @pl.loop(1, n_tp)
+    def _(k):
+        g = after_tp(k)
+
+        @pl.when(g < strips)
+        def _():
+            tp_copy(3, g, shp.at[g], shr.at[tp]).start()
+
+    def gated(total):
+        gate, up = total[:, :units], total[:, units:]
+        return (gate / (1.0 + jnp.exp(-gate)) * up).astype(BF)
+
+    @pl.when(tp < strips)
+    def _():
+        def gather(k, total):
+            src = before_tp(k)
+            landed(shr.at[src], tp_recv.at[3, src])
+            return total + shr[src].astype(F32)
+
+        hidden = gated(lax.fori_loop(1, n_tp, gather, shp[tp].astype(F32)))
+        shs[...] = hidden
+        shh[tp] = hidden
+
+        @pl.loop(1, n_tp)
+        def _(k):
+            g = after_tp(k)
+            tp_copy(4, g, shs, shh.at[tp]).start()
+
+    @pl.loop(1, n_sp)
+    def _(k):
+        src = (sp + n_sp - k) % n_sp
+        landed(dsp_in.at[src], sp_recv.at[0, src])
+
+    flat = dsp_in[...].astype(F32).reshape(seats, LANES).astype(BF)
+    xbuf[...] = dot(smat[...], flat).reshape(local, quarters * share, LANES).astype(BF)
+
+    @pl.loop(0, local)
+    def _(i):
+        e = (tp // quarters + i) % local
+        x = xbuf[e]
+        for half, weights in ((0, eg), (1, eu)):
+            made = dot(x, weights[e]).astype(BF).astype(F32)
+            for q in range(quarters):
+                gp[quarters * e + q, :, half * units : (half + 1) * units] = made[q * share : (q + 1) * share].astype(BF)
+
+        @pl.loop(0, quarters)
+        def _(q):
+            g = quarters * e + (tp + q) % quarters
+
+            @pl.when(g != tp)
+            def _():
+                tp_copy(5, g, gp.at[g], gin.at[tp]).start()
+
+    def gather_gate(k, total):
+        src = before_tp(k)
+        landed(gin.at[src], tp_recv.at[5, src])
+        return total + gin[src].astype(F32)
+
+    hidden = gated(lax.fori_loop(1, n_tp, gather_gate, gp[tp].astype(F32)))
+    hs[...] = hidden
+    hin[tp] = hidden
+
+    @pl.loop(1, n_tp)
+    def _(k):
+        g = after_tp(k)
+        tp_copy(6, g, hs, hin.at[tp]).start()
+
+    @pl.loop(0, strips)
+    def _(src):
+        @pl.when(src != tp)
+        def _():
+            landed(shh.at[src], tp_recv.at[4, src])
+
+    shared_out = dot(shh[...].reshape(rows, units), sd[...])
+
+    @pl.loop(1, n_tp)
+    def _(k):
+        src = before_tp(k)
+        landed(hin.at[src], tp_recv.at[6, src])
+
+    for e in range(local):
+        h = jnp.concatenate([hin[quarters * e + q].astype(F32) for q in range(quarters)], axis=0).astype(BF)
+        obuf[e * quarters * share : (e + 1) * quarters * share, :] = dot(h, ed[e]).astype(BF)
+    ret_out[...] = dot(rmat[...], obuf[...]).reshape(n_sp, PADDED, LANES).astype(BF)
+
+    @pl.loop(1, n_sp)
+    def _(k):
+        d = (sp + k) % n_sp
+        sp_copy(1, d, ret_out.at[d], ret_in.at[sp]).start()
+
+    ret_in[sp] = ret_out[sp]
+
+    @pl.loop(1, n_sp)
+    def _(k):
+        src = (sp + n_sp - k) % n_sp
+        landed(ret_in.at[src], sp_recv.at[1, src])
+
+    flat = ret_in[...].astype(F32).reshape(seats, LANES).astype(BF)
+    routed = gates[:, 0:1] * dot(oh[0], flat) + gates[:, 1:2] * dot(oh[1], flat)
+    out[...] = (stream + (routed + shared_out)).astype(BF)
+
+    @pl.loop(1, n_tp)
+    def _(k):
+        g = after_tp(k)
+        tp_copy(0, g, part.at[g], rs.at[tp]).wait_send()
+        tp_copy(1, g, sts.at[0], st.at[0, tp]).wait_send()
+        tp_copy(2, g, sts.at[1], st.at[1, tp]).wait_send()
+
+        @pl.when(g < strips)
+        def _():
+            tp_copy(3, g, shp.at[g], shr.at[tp]).wait_send()
+
+        @pl.when(tp < strips)
+        def _():
+            tp_copy(4, g, shs, shh.at[tp]).wait_send()
+
+        tp_copy(5, g, gp.at[g], gin.at[tp]).wait_send()
+        tp_copy(6, g, hs, hin.at[tp]).wait_send()
+
+    @pl.loop(1, n_sp)
+    def _(k):
+        d = (sp + k) % n_sp
+        sp_copy(0, d, dsp_out.at[d], dsp_in.at[sp]).wait_send()
+        sp_copy(1, d, ret_out.at[d], ret_in.at[sp]).wait_send()
+
+
+def rest(attended, *arrays):
+    out_a, out_b, resid, mix_gain, ffn_gain, routes, gates, exp_gate, exp_up, exp_down, sh_gate, sh_up, sh_down = arrays
+    n_sp, n_tp = lax.axis_size("sp"), lax.axis_size("tp")
+    rows = resid.shape[0]
+    local, _, units = exp_gate.shape
+    used = n_sp * CAP
+    share = local * used // n_tp
+    strips = rows // 16
+    seats = n_sp * PADDED
+    e, s, c = np.meshgrid(np.arange(local), np.arange(n_sp), np.arange(CAP), indexing="ij")
+    tcol = (s * PADDED + e * CAP + c).reshape(-1, 1).astype(np.int32)
+    rcol = np.full((seats, 1), -1, np.int32)
+    rcol[tcol[:, 0], 0] = np.arange(local * used)
+    dma = pltpu.SemaphoreType.DMA
+    vmem = pltpu.VMEM
+    return pl.pallas_call(
+        functools.partial(rest_kernel, n_sp, n_tp),
+        out_shape=jax.ShapeDtypeStruct((rows, LANES), BF),
+        in_specs=[pl.BlockSpec(memory_space=pltpu.VMEM)] * 16,
+        out_specs=pl.BlockSpec(memory_space=pltpu.VMEM),
+        scratch_shapes=[
+            vmem((n_tp, rows, LANES), BF),
+            vmem((n_tp, rows, LANES), BF),
+            vmem((2, 8, 2 * LANES), F32),
+            vmem((2, n_tp, 8, 2 * LANES), F32),
+            vmem((n_sp, PADDED, LANES), BF),
+            vmem((n_sp, PADDED, LANES), BF),
+            vmem((n_sp, PADDED, LANES), BF),
+            vmem((n_sp, PADDED, LANES), BF),
+            vmem((strips, 16, 2 * units), BF),
+            vmem((n_tp, 16, 2 * units), BF),
+            vmem((16, units), BF),
+            vmem((strips, 16, units), BF),
+            vmem((local, used, LANES), BF),
+            vmem((n_tp, share, 2 * units), BF),
+            vmem((n_tp, share, 2 * units), BF),
+            vmem((share, units), BF),
+            vmem((n_tp, share, units), BF),
+            vmem((local * used, LANES), BF),
+            vmem((2, rows, seats), BF),
+            vmem((local * used, seats), BF),
+            vmem((seats, local * used), BF),
+            dma((7, n_tp)),
+            dma((7, n_tp)),
+            dma((2, n_sp)),
+            dma((2, n_sp)),
+        ],
+        compiler_params=pltpu.CompilerParams(
+            collective_id=1, has_side_effects=True, vmem_limit_bytes=48 * 1024 * 1024),
+    )(attended, out_a, out_b, resid, mix_gain.reshape(1, -1), ffn_gain.reshape(1, -1), routes, gates,
+      exp_gate, exp_up, exp_down, sh_gate, sh_up, sh_down, jnp.asarray(tcol), jnp.asarray(rcol))
 
 
 def shards(query_a, key_a, value_a, query_b, key_b, value_b, stop_a, stop_b, *others):

time: 342 us -> 164 us (0.48)
  waiting for transfers between devices: 149 us -> 0 us
  Pallas kernels: 42 us -> 146 us
  blocking collectives: 59 us -> 0 us
  starting transfers between devices: 55.2 us -> 0 us
  between operations: 13.8 us -> 0.14 us
  matrix products: 7.99 us -> 0 us
  local copies, waits for them, and re-layouts: 12 us -> 16.5 us
    psum x1 -> x0, waiting for transfers between devices: 106 us -> none  [rest(): up_pre = lax.psum(up_part.astype(BF), 'tp').astype(F32)]
    pallas_call x0 -> x1, Pallas kernels: none -> 104 us  [rest(): pl.pallas_call(functools.partial(rest_kernel, n_sp, n_tp), out_shape=jax....]
    psum x2 -> x0, blocking collectives: 59 us -> none  [the longest x1 29.5 us: rest(): mix_total = lax.psum(jnp.sum(mixed * mixed, axis=1), 'tp')]
    all_to_all x3 -> x0, starting transfers between devices: 55.2 us -> none  [the longest x1 33.7 us: rest(): lax.all_to_all(outgoing, 'sp', split_axis=0, concat_axis=0, tiled=True)]
    all_to_all x3 -> x0, waiting for transfers between devices: 42.8 us -> none  [the longest x1 16.5 us: rest(): lax.all_to_all(produced.astype(BF), 'sp', split_axis=0, concat_axis=0, ti...]
    unnamed x46 -> x43, local copies, waits for them, and re-layouts: 6.73 us -> 16.5 us
    dot_general x9 -> x0, matrix products: 7.99 us -> none  [the longest x5 3.46 us: dot(): return jnp.dot(a, b, preferred_element_type=F32)]
  transfers between devices with their start and end apart: 4 -> 0, of which waited for: 4 -> 0; matrix products, arithmetic and copies ran while one was open for 1% -> 0% of each run, Pallas kernels for 0% -> 0%
where the time goes in v2:
time: 164 us; the launch traced here: 163 us
  Pallas kernels  146 us (89%)
  local copies, waits for them, and re-layouts  16.5 us (10%)
    pallas_call x1, Pallas kernels, rest(): pl.pallas_call(functools.partial(rest_kernel, n_sp, n_tp), out_shape=jax....  104 us
    pallas_call x1, Pallas kernels, attention(): pl.pallas_call(functools.partial(attention_kernel, nz), out_shape=jax.Sha...  42 us
    unnamed x43, local copies, waits for them, and re-layouts  16.5 us

profile of v2, /device:TPU:1, one launch (start us, length us, event | category | flops | bytes accessed | tf_op | source)
XLA Modules:
  0.0 163.0 jit_solution(12518412648865863472)
XLA Ops:
  0.0 0.0 copy-start
  0.0 0.8 copy.24.sa
  0.9 0.8 copy.25.sb
  1.7 0.0 copy-start.11
  1.7 0.8 copy-done.11
  2.5 0.0 copy-start.12
  2.5 0.8 copy-done.12
  3.3 0.0 copy-start.13
  3.3 0.8 copy-done.13
  4.1 0.0 copy-start.14
  4.1 0.8 copy-done.14
  4.9 0.0 copy-start.15
  4.9 0.8 copy-done.15
  5.7 0.0 copy-start.16
  5.7 0.8 copy-done.16
  6.5 0.0 copy-start.5
  6.5 42.0 %shard_map.217.att = bf16[192,256]{1,0:T(8,128)(2,1)S(1)} custom-call(bf16[192,128]{1,0:T(8,128)(2,1)S(1)} %copy-done.11, bf16[192,128]{1,0:T(8,128)(2,1)S(1)} %copy-done.12, bf16[192,128]{1,0:T(8,128)(2,1)S(1)} %copy-done.13, bf16[192,128]{1,0:T(8,128)(2,1)S(1)} %copy-done.14, bf16[192,128]{1,0:T(8,128)(2,1)S(1)} %copy-done.15, ...), custom_call_target="tpu_custom_call" | custom-call | tf_op jit(solution)/shard_map/pallas_call | solution.py:251
  48.5 0.8 copy.26.routes
  49.3 0.0 copy-start.10
  49.3 0.0 copy-start.17
  49.3 0.0 copy-start.18
  49.3 0.8 copy.27.gates
  50.1 0.0 copy-done
  50.1 0.0 copy-done.5
  50.2 0.0 copy-done.10
  50.2 0.0 copy-done.17
  50.2 0.0 copy-done.18
  50.2 0.0 copy-start.1
  50.2 1.0 copy-done.1
  51.2 0.0 copy-start.2
  51.2 1.0 copy-done.2
  52.3 0.0 copy-start.3
  52.3 1.0 copy-done.3
  53.3 0.0 copy-start.4
  53.3 1.0 copy-done.4
  54.4 0.0 copy-start.6
  54.4 1.0 copy-done.6
  55.3 0.0 copy-start.7
  55.3 0.9 copy-done.7
  56.2 0.0 copy-start.8
  56.2 0.9 copy-done.8
  57.1 0.0 copy-start.9
  57.1 0.9 copy-done.9
  58.0 104.4 %shard_map.218 = bf16[192,128]{1,0:T(8,128)(2,1)S(1)} custom-call(bf16[192,256]{1,0:T(8,128)(2,1)S(1)} %shard_map.217.att, bf16[128,2048]{1,0:T(8,128)(2,1)S(1)} %copy-done, bf16[128,2048]{1,0:T(8,128)(2,1)S(1)} %copy-done.1, bf16[192,128]{1,0:T(8,128)(2,1)S(1)} %copy-done.10, f32[1,128]{1,0:T(1,128)S(1)} %bitcast.2, f32[1,128]{1,0:T(1,128)S(1)} %bitcast.3, ...), custom_call_target="tpu_custom_call" | custom-call | tf_op jit(solution)/shard_map/pallas_call | solution.py:544
  162.4 0.6 copy.29
Async XLA Ops:
  0.0 50.1 %copy-start = (bf16[128,2048]{1,0:T(8,128)(2,1)S(1)}, bf16[128,2048]{1,0:T(8,128)(2,1)}, u32[]{:S(2)}) copy-start(bf16[128,2048]{1,0:T(8,128)(2,1)} %oa.1) | copy-start | bytes 1572868
  1.7 0.8 copy-start.11
  2.5 0.8 copy-start.12
  3.3 0.8 copy-start.13
  4.1 0.8 copy-start.14
  4.9 0.8 copy-start.15
  5.7 0.8 copy-start.16
  6.5 43.7 %copy-start.5 = (s32[768,1]{1,0:T(8,128)S(1)}, s32[768,1]{1,0:T(8,128)}, u32[]{:S(2)}) copy-start(s32[768,1]{1,0:T(8,128)} %constant.5.clone.rcol) | copy-start | bytes 9220
  49.3 0.9 copy-start.10
  49.3 0.9 copy-start.17
  49.3 0.9 copy-start.18
  50.2 1.0 copy-start.1
  51.2 1.0 copy-start.2
  52.3 1.0 copy-start.3
  53.3 1.0 copy-start.4
  54.4 1.0 copy-start.6
  55.3 0.9 copy-start.7
  56.2 0.9 copy-start.8
  57.1 0.9 copy-start.9

commit v3 on v1

v3 whole, which is shorter than its diff:
```python
import functools

import jax
import jax.numpy as jnp
from jax import lax
from jax.experimental import pallas as pl
from jax.experimental.pallas import tpu as pltpu
from jax.sharding import PartitionSpec as P

D = 2048
EPS = 1e-06
MESH = pl.DeviceIdType.MESH
BF = jnp.bfloat16
F32 = jnp.float32
LANES = 128
CAP = 5
PADDED = 24


def dot(a, b):
    return jnp.dot(a, b, preferred_element_type=F32)


def softplus_block(query, keys, stop, scale, later, valid):
    scores = lax.dot_general(query, keys, (((1,), (1,)), ((), ())), preferred_element_type=F32)
    z = scores * scale + stop
    sp = jnp.maximum(z, 0.0) + jnp.log(1.0 + jnp.exp(-jnp.abs(z)))
    if valid is not None:
        sp = jnp.where(valid, sp, 0.0)
    after = dot(sp.astype(BF), later)
    weight = jnp.exp(z - sp - after)
    if valid is not None:
        weight = jnp.where(valid, weight, 0.0)
    return weight.astype(BF), jnp.sum(sp, axis=1, keepdims=True)


def layer_kernel(n_sp, n_tp, *refs):
    (qa_h, ka_h, va_h, qb_h, kb_h, vb_h, sa_h, sb_h, oa_h, ob_h, resid_h, mg_h, fg_h, routes_h, gates_h,
     eg, eu, ed_h, sg_h, su_h, sd_h, out,
     qa, ka, va, qb, kb, vb, sa, sb, oa, ob, resid, mg, fg, routes, gates, ed, sg, su, sd,
     buf, accn, accf, ln, later,
     part, rs, sts, st, dsp_out, dsp_in, ret_out, ret_in, shp, shr, shs, shh, xbuf, xin, wgu, hs, hin, obuf, oh,
     choose, smat, rmat,
     lsem, ssu, rsu, ssd, rsd, ssp, rsp, wsend, wrecv, wloc, tp_send, tp_recv, sp_send, sp_recv) = refs
    rows = resid.shape[0]
    local, units = ed.shape[0], ed.shape[1]
    quarters = n_tp // local
    used = n_sp * CAP
    seats = n_sp * PADDED
    strips = rows // 16
    wide = 2 * LANES
    nz = n_sp // 2
    up_steps = nz // 2
    down_steps = nz - 1 - up_steps
    last_far = nz - 2 - up_steps
    sp = lax.axis_index("sp")
    tp = lax.axis_index("tp")
    z = sp // 2
    c = sp % 2
    up_id = (2 * ((z + 1) % nz) + c, tp)
    down_id = (2 * ((z + nz - 1) % nz) + c, tp)
    pair_id = (2 * z + 1 - c, tp)
    drains = []

    barrier = pltpu.get_barrier_semaphore()

    @pl.loop(1, n_sp)
    def _(k):
        pl.semaphore_signal(barrier, inc=1, device_id=((sp + n_sp - k) % n_sp, tp), device_id_type=MESH)

    @pl.loop(1, n_tp)
    def _(k):
        pl.semaphore_signal(barrier, inc=1, device_id=(sp, (tp + k) % n_tp), device_id_type=MESH)

    staged = [
        (ka_h, ka), (va_h, va), (kb_h, kb), (vb_h, vb), (routes_h, routes), (qa_h, qa), (qb_h, qb), (sa_h, sa),
        (sb_h, sb), (oa_h, oa), (ob_h, ob), (resid_h, resid), (mg_h, mg), (fg_h, fg), (gates_h, gates),
        (ed_h, ed), (sg_h, sg), (su_h, su), (sd_h, sd)]
    loads = [pltpu.make_async_copy(a, b, lsem.at[i]) for i, (a, b) in enumerate(staged)]
    for load in loads:
        load.start()

    def column(ref, k):
        return jnp.transpose(jnp.broadcast_to(ref[k : k + 1, :].astype(F32), (LANES, rows)))

    span = 2 * rows
    j = lax.broadcasted_iota(jnp.int32, (span, span), 0)
    s = lax.broadcasted_iota(jnp.int32, (span, span), 1)
    later[...] = (j > s).astype(BF)
    accf[...] = jnp.zeros_like(accf)
    half = lax.broadcasted_iota(jnp.int32, (rows, LANES), 1) < LANES // 2

    def index_of(shape, dim):
        return lax.broadcasted_iota(jnp.int32, shape, dim).astype(F32)

    i = index_of((local * used, LANES), 0)
    e = jnp.floor((i + 0.5) * (1.0 / used))
    i = i - used * e
    g = jnp.floor((i + 0.5) * (1.0 / CAP))
    smat[...] = (index_of((local * used, seats), 1) == (g * PADDED + e * CAP + (i - CAP * g))[:, 0:1]).astype(BF)
    i = index_of((seats, LANES), 0)
    g = jnp.floor((i + 0.5) * (1.0 / PADDED))
    i = i - PADDED * g
    e = jnp.floor((i + 0.5) * (1.0 / CAP))
    target = jnp.where(e < local, e * used + g * CAP + (i - CAP * e), -1.0)
    rmat[...] = (index_of((seats, local * used), 1) == target[:, 0:1]).astype(BF)
    loads[4].wait()
    experts = local * n_sp
    e_at = index_of((rows, experts), 1)
    named_by = [column(routes, k) for k in range(2)]
    named = [e_at == named_by[k][:, 0:1] for k in range(2)]
    members = jnp.where(named[0] | named[1], 1.0, 0.0).astype(BF)
    prior = dot((index_of((rows, rows), 1) < index_of((rows, rows), 0)).astype(BF), members)
    hits = None
    for k in range(2):
        home = jnp.floor((named_by[k] + 0.5) * (1.0 / local))
        rank = jnp.sum(jnp.where(named[k], prior, 0.0), axis=1, keepdims=True)
        seat = home * PADDED + (named_by[k] - local * home) * CAP + rank
        oh[k] = (index_of((rows, seats), 1) == seat[:, 0:1]).astype(BF)
        tall = jnp.concatenate([seat, jnp.full((wide - rows, LANES), -1.0, F32)], axis=0)
        hit = index_of((seats, wide), 0) == jnp.transpose(tall)[0:1, :]
        hits = hit if hits is None else hits | hit
    choose[...] = hits.astype(BF)

    for load in loads[:4]:
        load.wait()
    pl.semaphore_wait(barrier, n_tp + n_sp - 2)

    mine = pl.ds(pl.multiple_of(c * rows, rows), rows)
    theirs = pl.ds(pl.multiple_of((1 - c) * rows, rows), rows)
    srcs = (ka, va, kb, vb)

    def place(block, a):
        return buf.at[block, a, mine, :]

    def other(block, a):
        return buf.at[block, a, theirs, :]

    def up_copy(step, a, src):
        return pltpu.make_async_remote_copy(
            src_ref=src, dst_ref=place(z + 1 - step, a), send_sem=ssu.at[step - 1, a], recv_sem=rsu.at[step - 1, a],
            device_id=up_id, device_id_type=MESH)

    def down_copy(step, a, src):
        return pltpu.make_async_remote_copy(
            src_ref=src, dst_ref=place((z + step - 1) % nz, a), send_sem=ssd.at[step - 1, a],
            recv_sem=rsd.at[step - 1, a], device_id=down_id, device_id_type=MESH)

    def pair_copy(index, block, a, src):
        return pltpu.make_async_remote_copy(
            src_ref=src, dst_ref=place(block, a), send_sem=ssp.at[index, a], recv_sem=rsp.at[index, a],
            device_id=pair_id, device_id_type=MESH)

    def landed(ref, sem):
        pltpu.make_async_copy(ref, ref, sem).wait()

    def sends_up(step):
        return (z < nz - 1) & (z + 1 - step >= 0)

    def sends_down(step):
        return (z + step - 1) % nz <= last_far

    def gets_up(step):
        return z - step >= 0

    def gets_down(step):
        return (z + step) % nz <= last_far

    def far(step):
        return z + step >= nz

    for a in range(4):
        @pl.when(sends_up(1))
        def _(a=a):
            up_copy(1, a, srcs[a]).start()

        @pl.when(sends_down(1))
        def _(a=a):
            down_copy(1, a, srcs[a]).start()

        pair_copy(0, z, a, srcs[a]).start()
        buf[z, a, mine, :] = srcs[a][...]

    def after_tp(k):
        return (tp + k) % n_tp

    def before_tp(k):
        return (tp + n_tp - k) % n_tp

    def weights_copy(h, g):
        src = (eg, eu)[h].at[g // quarters, :, pl.ds(pl.multiple_of((g % quarters) * LANES, LANES), LANES)]
        dst = wgu.at[tp, :, pl.ds(h * LANES, LANES)]
        return src, dst

    def weights_remote(h, g):
        src, dst = weights_copy(h, g)
        return pltpu.make_async_remote_copy(
            src_ref=src, dst_ref=dst, send_sem=wsend.at[h, g], recv_sem=wrecv.at[h, tp],
            device_id=(sp, g), device_id_type=MESH)

    @pl.loop(1, n_tp)
    def _(k):
        for h in range(2):
            weights_remote(h, after_tp(k)).start()

    for h in range(2):
        src, dst = weights_copy(h, tp)
        pltpu.make_async_copy(src, dst, wloc.at[h]).start()

    for load in loads[5:]:
        load.wait()
    qa_all = qa[...]
    zero = jnp.zeros_like(qa_all)
    qa_heads = (jnp.where(half, qa_all, zero), jnp.where(half, zero, qa_all))
    stops = [column(sa, 0)[:, 0:1], column(sa, 1)[:, 0:1], column(sb, 0)[:, 0:1]]

    def group_a(block, valid=None):
        keys = buf[block, 0]
        values = buf[block, 1]
        pieces = [softplus_block(qa_heads[h], keys, stops[h], 64 ** -0.5, later[...], valid) for h in range(2)]
        added = jnp.where(half, dot(pieces[0][0], values), dot(pieces[1][0], values))
        return added, jnp.where(half, pieces[0][1], pieces[1][1])

    def group_b(block, valid=None):
        weight, total = softplus_block(qb[...], buf[block, 2], stops[2], 128 ** -0.5, later[...], valid)
        return dot(weight, buf[block, 3]), jnp.broadcast_to(total, (rows, LANES))

    groups = (group_a, group_b)

    def cols(g):
        return slice(g * LANES, (g + 1) * LANES)

    def near(g, step):
        block = z - step
        for a in (2 * g, 2 * g + 1):
            landed(other(block, a), rsp.at[step, a])
        added, total = groups[g](block)
        accn[:, cols(g)] += jnp.exp(-ln[:, cols(g)]) * added
        ln[:, cols(g)] += total

    def distant(g, step):
        block = z + step - nz
        for a in (2 * g, 2 * g + 1):
            landed(other(block, a), rsp.at[up_steps + step, a])
        added, total = groups[g](block)
        accf[:, cols(g)] = jnp.exp(-total) * accf[:, cols(g)] + added

    def poll_up(step, a):
        @pl.when(gets_up(step))
        def _():
            ref = place(z - step, a)
            landed(ref, rsu.at[step - 1, a])

            @pl.when((step < up_steps) & (z < nz - 1))
            def _():
                up_copy(step + 1, a, ref).start()

            pair_copy(step, z - step, a, ref).start()

    def poll_down(step, a):
        @pl.when((step <= down_steps) & gets_down(step))
        def _():
            block = (z + step) % nz
            ref = place(block, a)
            landed(ref, rsd.at[step - 1, a])

            @pl.when(step < down_steps)
            def _():
                down_copy(step + 1, a, ref).start()

            @pl.when(far(step))
            def _():
                pair_copy(up_steps + step, block, a, ref).start()

    row_at = lax.broadcasted_iota(jnp.int32, (rows, span), 0) + c * rows
    key_at = lax.broadcasted_iota(jnp.int32, (rows, span), 1)
    valid = key_at < row_at
    for g in range(2):
        for a in (2 * g, 2 * g + 1):
            landed(other(z, a), rsp.at[0, a])
        added, total = groups[g](z, valid)
        accn[:, cols(g)] = added
        ln[:, cols(g)] = total
        for a in (2 * g, 2 * g + 1):
            poll_up(1, a)
            poll_down(1, a)

    @pl.loop(2, up_steps + 1)
    def _(step):
        before = step - 1
        for a in range(4):
            poll_up(step, a)
            poll_down(step, a)
            g = a // 2
            if a % 2 == 0:
                @pl.when(gets_up(before))
                def _():
                    near(g, before)
            else:
                @pl.when(far(before))
                def _():
                    distant(g, before)

    @pl.when(gets_up(up_steps))
    def _():
        for g in range(2):
            near(g, up_steps)

    att = (accn[...] + jnp.exp(-ln[...]) * accf[...]).astype(BF)

    @drains.append
    def _():
        for a in range(4):
            pair_copy(0, z, a, srcs[a]).wait_send()

        @pl.loop(1, up_steps + 1)
        def _(step):
            for a in range(4):
                @pl.when(sends_up(step))
                def _():
                    up_copy(step, a, place(z + 1 - step, a)).wait_send()

                @pl.when(gets_up(step))
                def _():
                    pair_copy(step, z - step, a, place(z - step, a)).wait_send()

        @pl.loop(1, down_steps + 1)
        def _(step):
            for a in range(4):
                @pl.when(sends_down(step))
                def _():
                    down_copy(step, a, place((z + step - 1) % nz, a)).wait_send()

                @pl.when(far(step))
                def _():
                    pair_copy(up_steps + step, z + step - nz, a, place(z + step - nz, a)).wait_send()

        @pl.loop(1, n_tp)
        def _(k):
            for h in range(2):
                weights_remote(h, after_tp(k)).wait_send()

    def tp_copy(phase, g, src, dst):
        return pltpu.make_async_remote_copy(
            src_ref=src, dst_ref=dst, send_sem=tp_send.at[phase, g], recv_sem=tp_recv.at[phase, tp],
            device_id=(sp, g), device_id_type=MESH)

    def sp_copy(phase, d, src, dst):
        return pltpu.make_async_remote_copy(
            src_ref=src, dst_ref=dst, send_sem=sp_send.at[phase, d], recv_sem=sp_recv.at[phase, sp],
            device_id=(d, tp), device_id_type=MESH)

    def tp_drain(phase, src, dst):
        @drains.append
        def _():
            @pl.loop(1, n_tp)
            def _(k):
                g = after_tp(k)
                tp_copy(phase, g, src(g), dst).wait_send()

    low, high = att[:, :LANES], att[:, LANES:]

    @pl.loop(1, n_tp + 1)
    def _(k):
        g = after_tp(k)
        strip = pl.ds(pl.multiple_of(g * LANES, LANES), LANES)
        part[g] = (dot(low, oa[:, strip]) + dot(high, ob[:, strip])).astype(BF)

        @pl.when(k < n_tp)
        def _():
            tp_copy(0, g, part.at[g], rs.at[tp]).start()

    tp_drain(0, lambda g: part.at[g], rs.at[tp])

    def gather_rs(k, total):
        src = before_tp(k)
        landed(rs.at[src], tp_recv.at[0, src])
        return total + rs[src].astype(F32)

    mixed = lax.fori_loop(1, n_tp, gather_rs, part[tp].astype(F32))

    gained = mixed * mg[...]
    x = resid[...].astype(F32)
    lane = lax.broadcasted_iota(jnp.int32, (rows, LANES), 1)
    own = jnp.zeros((rows, LANES), F32)
    for k, product in enumerate((mixed * mixed, x * x, x * gained, gained * gained)):
        own = jnp.where(lane == k, jnp.sum(product, axis=1, keepdims=True), own)
    lines = jnp.transpose(jnp.concatenate([own, jnp.zeros((wide - rows, LANES), F32)], axis=0))[0:8, :]
    sts[...] = lines

    @pl.loop(1, n_tp)
    def _(k):
        tp_copy(1, after_tp(k), sts, st.at[tp]).start()

    tp_drain(1, lambda g: sts, st.at[tp])

    def gather_st(k, total):
        src = before_tp(k)
        landed(st.at[src], tp_recv.at[1, src])
        return total + st[src]

    lines = lax.fori_loop(1, n_tp, gather_st, lines)
    total = jnp.transpose(jnp.concatenate([lines, jnp.zeros((LANES - 8, wide), F32)], axis=0))[:rows, :]
    scale = lax.rsqrt(total[:, 0:1] / D + EPS)
    square = total[:, 1:2] + scale * (2.0 * total[:, 2:3] + scale * total[:, 3:4])
    stream = (x + gained * scale).astype(BF).astype(F32)
    scale = lax.rsqrt(jnp.maximum(square, 0.0) / D + EPS)
    normed = (stream * scale * fg[...]).astype(BF)

    tall = jnp.concatenate([normed, jnp.zeros((wide - rows, LANES), BF)], axis=0)
    dsp_out[...] = dot(choose[...], tall).reshape(n_sp, PADDED, LANES).astype(BF)

    def sp_drain(phase, src, dst):
        @drains.append
        def _():
            @pl.loop(1, n_sp)
            def _(k):
                d = (sp + k) % n_sp
                sp_copy(phase, d, src.at[d], dst).wait_send()

    @pl.loop(1, n_sp)
    def _(k):
        d = (sp + k) % n_sp
        sp_copy(0, d, dsp_out.at[d], dsp_in.at[sp]).start()

    sp_drain(0, dsp_out, dsp_in.at[sp])
    dsp_in[sp] = dsp_out[sp]

    shp[:, :, :units] = dot(normed, sg[...]).reshape(strips, 16, units).astype(BF)
    shp[:, :, units:] = dot(normed, su[...]).reshape(strips, 16, units).astype(BF)

    @pl.loop(1, n_tp)
    def _(k):
        g = after_tp(k)

        @pl.when(g < strips)
        def _():
            tp_copy(2, g, shp.at[g], shr.at[tp]).start()

    def gated(gate, up):
        return (gate / (1.0 + jnp.exp(-gate)) * up).astype(BF)

    @pl.when(tp < strips)
    def _():
        def gather(k, total):
            src = before_tp(k)
            landed(shr.at[src], tp_recv.at[2, src])
            return total + shr[src].astype(F32)

        both = lax.fori_loop(1, n_tp, gather, shp[tp].astype(F32))
        hidden = gated(both[:, :units], both[:, units:])
        shs[...] = hidden
        shh[tp] = hidden

        @pl.loop(1, n_tp)
        def _(k):
            tp_copy(3, after_tp(k), shs, shh.at[tp]).start()

    @drains.append
    def _():
        @pl.loop(1, n_tp)
        def _(k):
            g = after_tp(k)

            @pl.when(g < strips)
            def _():
                tp_copy(2, g, shp.at[g], shr.at[tp]).wait_send()

            @pl.when(tp < strips)
            def _():
                tp_copy(3, g, shs, shh.at[tp]).wait_send()

    @pl.loop(1, n_sp)
    def _(k):
        src = (sp + n_sp - k) % n_sp
        landed(dsp_in.at[src], sp_recv.at[0, src])

    flat = dsp_in[...].astype(F32).reshape(seats, LANES).astype(BF)
    xbuf[...] = dot(smat[...], flat).reshape(local, used, LANES).astype(BF)

    @pl.loop(1, n_tp)
    def _(k):
        g = after_tp(k)
        tp_copy(4, g, xbuf.at[g // quarters], xin.at[tp]).start()

    tp_drain(4, lambda g: xbuf.at[g // quarters], xin.at[tp])
    for h in range(2):
        src, dst = weights_copy(h, tp)
        pltpu.make_async_copy(src, dst, wloc.at[h]).wait()

    def gather_x(k, total):
        src = before_tp(k)
        for h in range(2):
            landed(wgu.at[src, :, pl.ds(h * LANES, LANES)], wrecv.at[h, src])
        landed(xin.at[src], tp_recv.at[4, src])
        return total + dot(xin[src], wgu[src])

    both = lax.fori_loop(1, n_tp, gather_x, dot(xbuf[tp // quarters], wgu[tp]))
    hidden = gated(both[:, :LANES], both[:, LANES:])
    hs[...] = hidden
    hin[tp] = hidden

    @pl.loop(1, n_tp)
    def _(k):
        tp_copy(5, after_tp(k), hs, hin.at[tp]).start()

    tp_drain(5, lambda g: hs, hin.at[tp])

    @pl.loop(0, strips)
    def _(src):
        @pl.when(src != tp)
        def _():
            landed(shh.at[src], tp_recv.at[3, src])

    shared_out = dot(shh[...].reshape(rows, units), sd[...])

    @pl.loop(1, n_tp)
    def _(k):
        src = before_tp(k)
        landed(hin.at[src], tp_recv.at[5, src])

    for e in range(local):
        h = jnp.concatenate([hin[quarters * e + q] for q in range(quarters)], axis=1)
        obuf[e * used : (e + 1) * used, :] = dot(h, ed[e]).astype(BF)
    ret_out[...] = dot(rmat[...], obuf[...]).reshape(n_sp, PADDED, LANES).astype(BF)

    @pl.loop(1, n_sp)
    def _(k):
        d = (sp + k) % n_sp
        sp_copy(1, d, ret_out.at[d], ret_in.at[sp]).start()

    sp_drain(1, ret_out, ret_in.at[sp])
    ret_in[sp] = ret_out[sp]
    weights = [column(gates, k) for k in range(2)]

    @pl.loop(1, n_sp)
    def _(k):
        src = (sp + n_sp - k) % n_sp
        landed(ret_in.at[src], sp_recv.at[1, src])

    flat = ret_in[...].astype(F32).reshape(seats, LANES).astype(BF)
    routed = weights[0] * dot(oh[0], flat) + weights[1] * dot(oh[1], flat)
    out[...] = (stream + (routed + shared_out)).astype(BF)
    for drain in drains:
        drain()


def shards(query_a, key_a, value_a, query_b, key_b, value_b, stop_a, stop_b, out_a, out_b, resid, mix_gain, ffn_gain,
           routes, gates, exp_gate, exp_up, exp_down, sh_gate, sh_up, sh_down):
    n_sp, n_tp = lax.axis_size("sp"), lax.axis_size("tp")
    rows = resid.shape[0]
    local, _, units = exp_gate.shape
    used = n_sp * CAP
    strips = rows // 16
    seats = n_sp * PADDED
    nz = n_sp // 2
    up_steps = nz // 2
    down_steps = nz - 1 - up_steps
    operands = (
        query_a, key_a, value_a, query_b, key_b, value_b, stop_a.T, stop_b.T, out_a, out_b, resid,
        mix_gain.reshape(1, -1), ffn_gain.reshape(1, -1), routes.T, gates.T, exp_gate, exp_up, exp_down, sh_gate,
        sh_up, sh_down)
    dma = pltpu.SemaphoreType.DMA
    vmem = pltpu.VMEM
    held = [vmem(a.shape, a.dtype) for i, a in enumerate(operands) if i not in (15, 16)]
    return pl.pallas_call(
        functools.partial(layer_kernel, n_sp, n_tp),
        out_shape=jax.ShapeDtypeStruct((rows, LANES), BF),
        in_specs=[pl.BlockSpec(memory_space=pl.ANY)] * len(operands),
        out_specs=pl.BlockSpec(memory_space=pltpu.VMEM),
        scratch_shapes=held + [
            vmem((nz, 4, 2 * rows, LANES), BF),
            vmem((rows, 2 * LANES), F32),
            vmem((rows, 2 * LANES), F32),
            vmem((rows, 2 * LANES), F32),
            vmem((2 * rows, 2 * rows), BF),
            vmem((n_tp, rows, LANES), BF),
            vmem((n_tp, rows, LANES), BF),
            vmem((8, 2 * LANES), F32),
            vmem((n_tp, 8, 2 * LANES), F32),
            vmem((n_sp, PADDED, LANES), BF),
            vmem((n_sp, PADDED, LANES), BF),
            vmem((n_sp, PADDED, LANES), BF),
            vmem((n_sp, PADDED, LANES), BF),
            vmem((strips, 16, 2 * units), BF),
            vmem((n_tp, 16, 2 * units), BF),
            vmem((16, units), BF),
            vmem((strips, 16, units), BF),
            vmem((local, used, LANES), BF),
            vmem((n_tp, used, LANES), BF),
            vmem((n_tp, LANES, 2 * LANES), BF),
            vmem((used, LANES), BF),
            vmem((n_tp, used, LANES), BF),
            vmem((local * used, LANES), BF),
            vmem((2, rows, seats), BF),
            vmem((seats, 2 * LANES), BF),
            vmem((local * used, seats), BF),
            vmem((seats, local * used), BF),
            dma((len(held),)),
            dma((up_steps, 4)),
            dma((up_steps, 4)),
            dma((down_steps, 4)),
            dma((down_steps, 4)),
            dma((nz, 4)),
            dma((nz, 4)),
            dma((2, n_tp)),
            dma((2, n_tp)),
            dma((2,)),
            dma((6, n_tp)),
            dma((6, n_tp)),
            dma((2, n_sp)),
            dma((2, n_sp)),
        ],
        compiler_params=pltpu.CompilerParams(
            collective_id=0, has_side_effects=True, vmem_limit_bytes=56 * 1024 * 1024),
    )(*operands)


def solution(mesh):
    row, col, both = P("tp", None), P("tp"), P("sp", "tp")
    in_specs = (both,) * 8 + (
        row, row, both, col, col, P("sp", None), P("sp", None),
        P("sp", "tp", None), P("sp", "tp", None), P("sp", None, "tp"), row, row, P(None, "tp"))
    return jax.shard_map(shards, mesh=mesh, in_specs=in_specs, out_specs=both, check_vma=False)
```

time: 342 us -> 129 us (0.38)
  waiting for transfers between devices: 149 us -> 0 us
  Pallas kernels: 42 us -> 127 us
  blocking collectives: 59 us -> 0 us
  starting transfers between devices: 55.2 us -> 0 us
  between operations: 13.8 us -> 0.01 us
  local copies, waits for them, and re-layouts: 12 us -> 1.42 us
  matrix products: 7.99 us -> 0 us
    psum x1 -> x0, waiting for transfers between devices: 106 us -> none  [rest(): up_pre = lax.psum(up_part.astype(BF), 'tp').astype(F32)]
    pallas_call x1, Pallas kernels: 42 us -> 127 us  [shards(): pl.pallas_call(functools.partial(layer_kernel, n_sp, n_tp), out_shape=jax...]
    psum x2 -> x0, blocking collectives: 59 us -> none  [the longest x1 29.5 us: rest(): mix_total = lax.psum(jnp.sum(mixed * mixed, axis=1), 'tp')]
    all_to_all x3 -> x0, starting transfers between devices: 55.2 us -> none  [the longest x1 33.7 us: rest(): lax.all_to_all(outgoing, 'sp', split_axis=0, concat_axis=0, tiled=True)]
    all_to_all x3 -> x0, waiting for transfers between devices: 42.8 us -> none  [the longest x1 16.5 us: rest(): lax.all_to_all(produced.astype(BF), 'sp', split_axis=0, concat_axis=0, ti...]
    dot_general x9 -> x0, matrix products: 7.99 us -> none  [the longest x5 3.46 us: dot(): return jnp.dot(a, b, preferred_element_type=F32)]
    unnamed x46 -> x1, local copies, waits for them, and re-layouts: 6.73 us -> 1.42 us
  transfers between devices with their start and end apart: 4 -> 0, of which waited for: 4 -> 0; matrix products, arithmetic and copies ran while one was open for 1% -> 0% of each run, Pallas kernels for 0% -> 0%
where the time goes in v3:
time: 129 us; the launch traced here: 128 us
  Pallas kernels  127 us (98%)
  local copies, waits for them, and re-layouts  1.42 us (1%)
    pallas_call x1, Pallas kernels, shards(): pl.pallas_call(functools.partial(layer_kernel, n_sp, n_tp), out_shape=jax...  127 us

profile of v3, /device:TPU:1, one launch (start us, length us, event | category | flops | bytes accessed | tf_op | source)
XLA Modules:
  0.0 128.4 jit_solution(3207483575998802665)
XLA Ops:
  0.0 127.0 %shard_map.199 = bf16[192,128]{1,0:T(8,128)(2,1)} custom-call(bf16[192,128]{1,0:T(8,128)(2,1)} %refs_0_.1, bf16[192,128]{1,0:T(8,128)(2,1)} %refs_1_.1, bf16[192,128]{1,0:T(8,128)(2,1)} %refs_2_.1, bf16[192,128]{1,0:T(8,128)(2,1)} %refs_3_.1, bf16[192,128]{1,0:T(8,128)(2,1)} %refs_4_.1, bf16[192,128]{1,0:T(8,128)(2,1)} %refs_5_.1, f32[2,192]{1,0:T(2,128)} %bitcast.6, ...), custom_call_target="tpu_custom_call" | custom-call | tf_op jit(solution)/shard_map/pallas_call | solution.py:566
  127.0 1.4 %copy.23 = bf16[192,128]{1,0:T(8,128)(2,1)} copy(bf16[192,128]{1,0:T(8,128)(2,1)} %shard_map.199) | data formatting | bytes 98304

commit v4 on v3

--- a/solution.py
+++ b/solution.py
@@ -41,12 +41,16 @@
      buf, accn, accf, ln, later,
      part, rs, sts, st, dsp_out, dsp_in, ret_out, ret_in, shp, shr, shs, shh, xbuf, xin, wgu, hs, hin, obuf, oh,
      choose, smat, rmat,
-     lsem, ssu, rsu, ssd, rsd, ssp, rsp, wsend, wrecv, wloc, tp_send, tp_recv, sp_send, sp_recv) = refs
+     lsem, tokens, ssu, rsu, ssd, rsd, ssp, rsp, wsend, wrecv, wloc, tp_send, tp_recv, sp_send, sp_recv) = refs
     rows = resid.shape[0]
     local, units = ed.shape[0], ed.shape[1]
     quarters = n_tp // local
     used = n_sp * CAP
     seats = n_sp * PADDED
+    parts = 2
+    part_used = used // parts
+    part_seats = seats // parts
+    homes = n_sp // parts
     strips = rows // 16
     wide = 2 * LANES
     nz = n_sp // 2
@@ -64,13 +68,22 @@
 
     barrier = pltpu.get_barrier_semaphore()
 
-    @pl.loop(1, n_sp)
-    def _(k):
-        pl.semaphore_signal(barrier, inc=1, device_id=((sp + n_sp - k) % n_sp, tp), device_id_type=MESH)
-
-    @pl.loop(1, n_tp)
-    def _(k):
-        pl.semaphore_signal(barrier, inc=1, device_id=(sp, (tp + k) % n_tp), device_id_type=MESH)
+    side = quarters
+    row = [(sp, tp // side * side + (tp + k) % side) for k in range(1, side)]
+    column_peers = [(sp, (tp + side * k) % n_tp) for k in range(1, n_tp // side)]
+    across = [(2 * ((z + step) % nz) + 1 - c, tp) for step in (1, nz - 1)]
+    first = [up_id, down_id, pair_id] + across + row + column_peers
+    for peer in first:
+        pl.semaphore_signal(barrier, inc=1, device_id=peer, device_id_type=MESH)
+
+    def pass_on(which, peers):
+        for peer in peers:
+            pl.semaphore_signal(tokens.at[which], inc=1, device_id=peer, device_id_type=MESH)
+
+    def along(distance):
+        return [(2 * ((z + step) % nz) + c, tp) for step in (distance, nz - distance)]
+
+    rounds = [1 << r for r in range((nz // 4).bit_length())]
 
     staged = [
         (ka_h, ka), (va_h, va), (kb_h, kb), (vb_h, vb), (routes_h, routes), (qa_h, qa), (qb_h, qb), (sa_h, sa),
@@ -83,6 +96,67 @@
     def column(ref, k):
         return jnp.transpose(jnp.broadcast_to(ref[k : k + 1, :].astype(F32), (LANES, rows)))
 
+    for load in loads[:4]:
+        load.wait()
+    pl.semaphore_wait(barrier, len(first))
+    pass_on(0, row)
+    pass_on(1, along(rounds[0]))
+
+    mine = pl.ds(pl.multiple_of(c * rows, rows), rows)
+    theirs = pl.ds(pl.multiple_of((1 - c) * rows, rows), rows)
+    srcs = (ka, va, kb, vb)
+
+    def place(block, a):
+        return buf.at[block, a, mine, :]
+
+    def other(block, a):
+        return buf.at[block, a, theirs, :]
+
+    def up_copy(step, a, src):
+        return pltpu.make_async_remote_copy(
+            src_ref=src, dst_ref=place(z + 1 - step, a), send_sem=ssu.at[step - 1, a], recv_sem=rsu.at[step - 1, a],
+            device_id=up_id, device_id_type=MESH)
+
+    def down_copy(step, a, src):
+        return pltpu.make_async_remote_copy(
+            src_ref=src, dst_ref=place((z + step - 1) % nz, a), send_sem=ssd.at[step - 1, a],
+            recv_sem=rsd.at[step - 1, a], device_id=down_id, device_id_type=MESH)
+
+    def pair_copy(index, block, a, src):
+        return pltpu.make_async_remote_copy(
+            src_ref=src, dst_ref=place(block, a), send_sem=ssp.at[index, a], recv_sem=rsp.at[index, a],
+            device_id=pair_id, device_id_type=MESH)
+
+    def landed(ref, sem):
+        pltpu.make_async_copy(ref, ref, sem).wait()
+
+    def sends_up(step):
+        return (z < nz - 1) & (z + 1 - step >= 0)
+
+    def sends_down(step):
+        return (z + step - 1) % nz <= last_far
+
+    def gets_up(step):
+        return z - step >= 0
+
+    def gets_down(step):
+        return (z + step) % nz <= last_far
+
+    def far(step):
+        return z + step >= nz
+
+    for a in range(4):
+        @pl.when(sends_up(1))
+        def _(a=a):
+            up_copy(1, a, srcs[a]).start()
+
+        @pl.when(sends_down(1))
+        def _(a=a):
+            down_copy(1, a, srcs[a]).start()
+
+        pair_copy(0, z, a, srcs[a]).start()
+        buf[z, a, mine, :] = srcs[a][...]
+
     span = 2 * rows
     j = lax.broadcasted_iota(jnp.int32, (span, span), 0)
     s = lax.broadcasted_iota(jnp.int32, (span, span), 1)
@@ -93,17 +167,18 @@
     def index_of(shape, dim):
         return lax.broadcasted_iota(jnp.int32, shape, dim).astype(F32)
 
-    i = index_of((local * used, LANES), 0)
-    e = jnp.floor((i + 0.5) * (1.0 / used))
-    i = i - used * e
+    i = index_of((local * part_used, LANES), 0)
+    e = jnp.floor((i + 0.5) * (1.0 / part_used))
+    i = i - part_used * e
     g = jnp.floor((i + 0.5) * (1.0 / CAP))
-    smat[...] = (index_of((local * used, seats), 1) == (g * PADDED + e * CAP + (i - CAP * g))[:, 0:1]).astype(BF)
-    i = index_of((seats, LANES), 0)
+    seat = g * PADDED + e * CAP + (i - CAP * g)
+    smat[...] = (index_of((local * part_used, part_seats), 1) == seat[:, 0:1]).astype(BF)
+    i = index_of((part_seats, LANES), 0)
     g = jnp.floor((i + 0.5) * (1.0 / PADDED))
     i = i - PADDED * g
     e = jnp.floor((i + 0.5) * (1.0 / CAP))
-    target = jnp.where(e < local, e * used + g * CAP + (i - CAP * e), -1.0)
-    rmat[...] = (index_of((seats, local * used), 1) == target[:, 0:1]).astype(BF)
+    seat = jnp.where(e < local, e * part_used + g * CAP + (i - CAP * e), -1.0)
+    rmat[...] = (index_of((part_seats, local * part_used), 1) == seat[:, 0:1]).astype(BF)
     loads[4].wait()
     experts = local * n_sp
     e_at = index_of((rows, experts), 1)
@@ -122,64 +197,6 @@
         hits = hit if hits is None else hits | hit
     choose[...] = hits.astype(BF)
 
-    for load in loads[:4]:
-        load.wait()
-    pl.semaphore_wait(barrier, n_tp + n_sp - 2)
-
-    mine = pl.ds(pl.multiple_of(c * rows, rows), rows)
-    theirs = pl.ds(pl.multiple_of((1 - c) * rows, rows), rows)
-    srcs = (ka, va, kb, vb)
-
-    def place(block, a):
-        return buf.at[block, a, mine, :]
-
-    def other(block, a):
-        return buf.at[block, a, theirs, :]
-
-    def up_copy(step, a, src):
-        return pltpu.make_async_remote_copy(
-            src_ref=src, dst_ref=place(z + 1 - step, a), send_sem=ssu.at[step - 1, a], recv_sem=rsu.at[step - 1, a],
-            device_id=up_id, device_id_type=MESH)
-
-    def down_copy(step, a, src):
-        return pltpu.make_async_remote_copy(
-            src_ref=src, dst_ref=place((z + step - 1) % nz, a), send_sem=ssd.at[step - 1, a],
-            recv_sem=rsd.at[step - 1, a], device_id=down_id, device_id_type=MESH)
-
-    def pair_copy(index, block, a, src):
-        return pltpu.make_async_remote_copy(
-            src_ref=src, dst_ref=place(block, a), send_sem=ssp.at[index, a], recv_sem=rsp.at[index, a],
-            device_id=pair_id, device_id_type=MESH)
-
-    def landed(ref, sem):
-        pltpu.make_async_copy(ref, ref, sem).wait()
-
-    def sends_up(step):
-        return (z < nz - 1) & (z + 1 - step >= 0)
-
-    def sends_down(step):
-        return (z + step - 1) % nz <= last_far
-
-    def gets_up(step):
-        return z - step >= 0
-
-    def gets_down(step):
-        return (z + step) % nz <= last_far
-
-    def far(step):
-        return z + step >= nz
-
-    for a in range(4):
-        @pl.when(sends_up(1))
-        def _(a=a):
-            up_copy(1, a, srcs[a]).start()
-
-        @pl.when(sends_down(1))
-        def _(a=a):
-            down_copy(1, a, srcs[a]).start()
-
-        pair_copy(0, z, a, srcs[a]).start()
-        buf[z, a, mine, :] = srcs[a][...]
 
     def after_tp(k):
         return (tp + k) % n_tp
@@ -198,6 +215,8 @@
             src_ref=src, dst_ref=dst, send_sem=wsend.at[h, g], recv_sem=wrecv.at[h, tp],
             device_id=(sp, g), device_id_type=MESH)
 
+    pl.semaphore_wait(tokens.at[0], len(row))
+
     @pl.loop(1, n_tp)
     def _(k):
         for h in range(2):
@@ -209,6 +228,8 @@
 
     for load in loads[5:]:
         load.wait()
+    pl.semaphore_wait(tokens.at[1], 2)
+    pass_on(2, along(rounds[1]))
     qa_all = qa[...]
     zero = jnp.zeros_like(qa_all)
     qa_heads = (jnp.where(half, qa_all, zero), jnp.where(half, zero, qa_all))
@@ -284,6 +305,10 @@
         for a in (2 * g, 2 * g + 1):
             poll_up(1, a)
             poll_down(1, a)
+
+    for r in range(2, len(rounds)):
+        pl.semaphore_wait(tokens.at[r], 2)
+        pass_on(r + 1, along(rounds[r]))
 
     @pl.loop(2, up_steps + 1)
     def _(step):
@@ -306,6 +331,7 @@
         for g in range(2):
             near(g, up_steps)
 
+    pl.semaphore_wait(tokens.at[len(rounds)], 2)
     att = (accn[...] + jnp.exp(-ln[...]) * accf[...]).astype(BF)
 
     @drains.append
@@ -410,21 +436,29 @@
     tall = jnp.concatenate([normed, jnp.zeros((wide - rows, LANES), BF)], axis=0)
     dsp_out[...] = dot(choose[...], tall).reshape(n_sp, PADDED, LANES).astype(BF)
 
-    def sp_drain(phase, src, dst):
-        @drains.append
-        def _():
-            @pl.loop(1, n_sp)
-            def _(k):
-                d = (sp + k) % n_sp
-                sp_copy(phase, d, src.at[d], dst).wait_send()
-
-    @pl.loop(1, n_sp)
-    def _(k):
-        d = (sp + k) % n_sp
-        sp_copy(0, d, dsp_out.at[d], dsp_in.at[sp]).start()
-
-    sp_drain(0, dsp_out, dsp_in.at[sp])
-    dsp_in[sp] = dsp_out[sp]
+    def near_first(body):
+        @pl.loop(0, nz)
+        def _(k):
+            reach = (k + 1) // 2
+            away = (z + nz + reach * (2 * (k % 2) - 1)) % nz
+            body(2 * away + 1 - c)
+
+            @pl.when(k > 0)
+            def _():
+                body(2 * away + c)
+
+    def berth(src, dst):
+        return 2 * ((src // 2 + nz + nz // 4 - dst // 2) % nz) + src % 2
+
+    def tenant(place):
+        return 2 * ((z + nz - nz // 4 + place // 2) % nz) + place % 2
+
+    def dispatch(d):
+        return sp_copy(0, d, dsp_out.at[d], dsp_in.at[berth(sp, d)])
+
+    near_first(lambda d: dispatch(d).start())
+    drains.append(lambda: near_first(lambda d: dispatch(d).wait_send()))
+    dsp_in[berth(sp, sp)] = dsp_out[sp]
 
     shp[:, :, :units] = dot(normed, sg[...]).reshape(strips, 16, units).astype(BF)
     shp[:, :, units:] = dot(normed, su[...]).reshape(strips, 16, units).astype(BF)
@@ -436,25 +470,6 @@
         @pl.when(g < strips)
         def _():
             tp_copy(2, g, shp.at[g], shr.at[tp]).start()
-
-    def gated(gate, up):
-        return (gate / (1.0 + jnp.exp(-gate)) * up).astype(BF)
-
-    @pl.when(tp < strips)
-    def _():
-        def gather(k, total):
-            src = before_tp(k)
-            landed(shr.at[src], tp_recv.at[2, src])
-            return total + shr[src].astype(F32)
-
-        both = lax.fori_loop(1, n_tp, gather, shp[tp].astype(F32))
-        hidden = gated(both[:, :units], both[:, units:])
-        shs[...] = hidden
-        shh[tp] = hidden
-
-        @pl.loop(1, n_tp)
-        def _(k):
-            tp_copy(3, after_tp(k), shs, shh.at[tp]).start()
 
     @drains.append
     def _():
@@ -470,41 +485,114 @@
             def _():
                 tp_copy(3, g, shs, shh.at[tp]).wait_send()
 
-    @pl.loop(1, n_sp)
-    def _(k):
-        src = (sp + n_sp - k) % n_sp
-        landed(dsp_in.at[src], sp_recv.at[0, src])
-
-    flat = dsp_in[...].astype(F32).reshape(seats, LANES).astype(BF)
-    xbuf[...] = dot(smat[...], flat).reshape(local, used, LANES).astype(BF)
-
-    @pl.loop(1, n_tp)
-    def _(k):
-        g = after_tp(k)
-        tp_copy(4, g, xbuf.at[g // quarters], xin.at[tp]).start()
-
-    tp_drain(4, lambda g: xbuf.at[g // quarters], xin.at[tp])
+    def gated(gate, up):
+        return (gate / (1.0 + jnp.exp(-gate)) * up).astype(BF)
+
+    def reduce_shared():
+        @pl.when(tp < strips)
+        def _():
+            def gather(k, total):
+                src = before_tp(k)
+                landed(shr.at[src], tp_recv.at[2, src])
+                return total + shr[src].astype(F32)
+
+            both = lax.fori_loop(1, n_tp, gather, shp[tp].astype(F32))
+            hidden = gated(both[:, :units], both[:, units:])
+            shs[...] = hidden
+            shh[tp] = hidden
+
+            @pl.loop(1, n_tp)
+            def _(k):
+                tp_copy(3, after_tp(k), shs, shh.at[tp]).start()
+
+    def send_rows(p):
+        @pl.loop(p * homes, (p + 1) * homes)
+        def _(place):
+            src = tenant(place)
+
+            @pl.when(src != sp)
+            def _():
+                landed(dsp_in.at[place], sp_recv.at[0, src])
+
+        flat = dsp_in[p * homes : (p + 1) * homes].astype(F32).reshape(part_seats, LANES).astype(BF)
+        xbuf[p] = dot(smat[...], flat).reshape(local, part_used, LANES).astype(BF)
+        xin[p, tp] = xbuf[p, tp // quarters]
+
+        @pl.loop(1, n_tp)
+        def _(k):
+            g = after_tp(k)
+            tp_copy(4 + p, g, xbuf.at[p, g // quarters], xin.at[p, tp]).start()
+
+        tp_drain(4 + p, lambda g: xbuf.at[p, g // quarters], xin.at[p, tp])
+
+    def send_hidden(p):
+        @pl.loop(1, n_tp)
+        def _(k):
+            src = before_tp(k)
+            landed(xin.at[p, src], tp_recv.at[4 + p, src])
+
+        x = jnp.concatenate([xin[p, g] for g in range(n_tp)], axis=1)
+        both = dot(x, wgu[...].reshape(n_tp * LANES, 2 * LANES))
+        hidden = gated(both[:, :LANES], both[:, LANES:])
+        hs[p] = hidden
+        hin[p, tp] = hidden
+
+        @pl.loop(1, n_tp)
+        def _(k):
+            tp_copy(4 + parts + p, after_tp(k), hs.at[p], hin.at[p, tp]).start()
+
+        tp_drain(4 + parts + p, lambda g: hs.at[p], hin.at[p, tp])
+
+    def giving(place):
+        d = tenant(place)
+        return sp_copy(1, d, ret_out.at[place], ret_in.at[sp])
+
+    def send_back(p):
+        @pl.loop(1, n_tp)
+        def _(k):
+            src = before_tp(k)
+            landed(hin.at[p, src], tp_recv.at[4 + parts + p, src])
+
+        for e in range(local):
+            h = jnp.concatenate([hin[p, quarters * e + q] for q in range(quarters)], axis=1)
+            obuf[e * part_used : (e + 1) * part_used, :] = dot(h, ed[e]).astype(BF)
+        made = dot(rmat[...], obuf[...]).reshape(homes, PADDED, LANES).astype(BF)
+        ret_out[p * homes : (p + 1) * homes] = made
+
+        @pl.loop(p * homes, (p + 1) * homes)
+        def _(place):
+            @pl.when(tenant(place) != sp)
+            def _():
+                giving(place).start()
+
+    @drains.append
+    def _():
+        @pl.loop(0, n_sp)
+        def _(place):
+            @pl.when(tenant(place) != sp)
+            def _():
+                giving(place).wait_send()
+
+    send_rows(0)
+    reduce_shared()
     for h in range(2):
         src, dst = weights_copy(h, tp)
         pltpu.make_async_copy(src, dst, wloc.at[h]).wait()
 
-    def gather_x(k, total):
+    @pl.loop(1, n_tp)
+    def _(k):
         src = before_tp(k)
         for h in range(2):
             landed(wgu.at[src, :, pl.ds(h * LANES, LANES)], wrecv.at[h, src])
-        landed(xin.at[src], tp_recv.at[4, src])
-        return total + dot(xin[src], wgu[src])
-
-    both = lax.fori_loop(1, n_tp, gather_x, dot(xbuf[tp // quarters], wgu[tp]))
-    hidden = gated(both[:, :LANES], both[:, LANES:])
-    hs[...] = hidden
-    hin[tp] = hidden
-
-    @pl.loop(1, n_tp)
-    def _(k):
-        tp_copy(5, after_tp(k), hs, hin.at[tp]).start()
-
-    tp_drain(5, lambda g: hs, hin.at[tp])
+
+    for p in range(1, parts):
+        send_rows(p)
+        send_hidden(p - 1)
+    send_hidden(parts - 1)
+    for p in range(parts):
+        send_back(p)
+    ret_in[sp] = ret_out[berth(sp, sp)]
+    weights = [column(gates, k) for k in range(2)]
 
     @pl.loop(0, strips)
     def _(src):
@@ -513,25 +601,6 @@
             landed(shh.at[src], tp_recv.at[3, src])
 
     shared_out = dot(shh[...].reshape(rows, units), sd[...])
-
-    @pl.loop(1, n_tp)
-    def _(k):
-        src = before_tp(k)
-        landed(hin.at[src], tp_recv.at[5, src])
-
-    for e in range(local):
-        h = jnp.concatenate([hin[quarters * e + q] for q in range(quarters)], axis=1)
-        obuf[e * used : (e + 1) * used, :] = dot(h, ed[e]).astype(BF)
-    ret_out[...] = dot(rmat[...], obuf[...]).reshape(n_sp, PADDED, LANES).astype(BF)
-
-    @pl.loop(1, n_sp)
-    def _(k):
-        d = (sp + k) % n_sp
-        sp_copy(1, d, ret_out.at[d], ret_in.at[sp]).start()
-
-    sp_drain(1, ret_out, ret_in.at[sp])
-    ret_in[sp] = ret_out[sp]
-    weights = [column(gates, k) for k in range(2)]
 
     @pl.loop(1, n_sp)
     def _(k):
@@ -553,6 +622,7 @@
     used = n_sp * CAP
     strips = rows // 16
     seats = n_sp * PADDED
+    parts = 2
     nz = n_sp // 2
     up_steps = nz // 2
     down_steps = nz - 1 - up_steps
@@ -586,17 +656,18 @@
             vmem((n_tp, 16, 2 * units), BF),
             vmem((16, units), BF),
             vmem((strips, 16, units), BF),
-            vmem((local, used, LANES), BF),
-            vmem((n_tp, used, LANES), BF),
+            vmem((parts, local, used // parts, LANES), BF),
+            vmem((parts, n_tp, used // parts, LANES), BF),
             vmem((n_tp, LANES, 2 * LANES), BF),
-            vmem((used, LANES), BF),
-            vmem((n_tp, used, LANES), BF),
-            vmem((local * used, LANES), BF),
+            vmem((parts, used // parts, LANES), BF),
+            vmem((parts, n_tp, used // parts, LANES), BF),
+            vmem((local * used // parts, LANES), BF),
             vmem((2, rows, seats), BF),
             vmem((seats, 2 * LANES), BF),
-            vmem((local * used, seats), BF),
-            vmem((seats, local * used), BF),
+            vmem((local * used // parts, seats // parts), BF),
+            vmem((seats // parts, local * used // parts), BF),
             dma((len(held),)),
+            pltpu.SemaphoreType.REGULAR(((nz // 4).bit_length() + 1,)),
             dma((up_steps, 4)),
             dma((up_steps, 4)),
             dma((down_steps, 4)),
@@ -606,8 +677,8 @@
             dma((2, n_tp)),
             dma((2, n_tp)),
             dma((2,)),
-            dma((6, n_tp)),
-            dma((6, n_tp)),
+            dma((4 + 2 * parts, n_tp)),
+            dma((4 + 2 * parts, n_tp)),
             dma((2, n_sp)),
             dma((2, n_sp)),
         ],

time: 129 us -> 122 us (0.946)
  Pallas kernels: 127 us -> 120 us
    pallas_call x1, Pallas kernels: 127 us -> 120 us  [shards(): pl.pallas_call(functools.partial(layer_kernel, n_sp, n_tp), out_shape=jax...]
where the time goes in v4:
time: 122 us
  Pallas kernels  120 us (98%)
  local copies, waits for them, and re-layouts  1.42 us (1%)
    pallas_call x1, Pallas kernels, shards(): pl.pallas_call(functools.partial(layer_kernel, n_sp, n_tp), out_shape=jax...  120 us

profile of v4, /device:TPU:1, one launch (start us, length us, event | category | flops | bytes accessed | tf_op | source)
XLA Modules:
  0.0 121.7 jit_solution(14611323896559140521)
XLA Ops:
  0.0 120.2 %shard_map.199 = bf16[192,128]{1,0:T(8,128)(2,1)} custom-call(bf16[192,128]{1,0:T(8,128)(2,1)} %refs_0_.1, bf16[192,128]{1,0:T(8,128)(2,1)} %refs_1_.1, bf16[192,128]{1,0:T(8,128)(2,1)} %refs_2_.1, bf16[192,128]{1,0:T(8,128)(2,1)} %refs_3_.1, bf16[192,128]{1,0:T(8,128)(2,1)} %refs_4_.1, bf16[192,128]{1,0:T(8,128)(2,1)} %refs_5_.1, f32[2,192]{1,0:T(2,128)} %bitcast.6, ...), custom_call_target="tpu_custom_call" | custom-call | tf_op jit(solution)/shard_map/pallas_call | solution.py:636
  120.2 1.4 %copy.23 = bf16[192,128]{1,0:T(8,128)(2,1)} copy(bf16[192,128]{1,0:T(8,128)(2,1)} %shard_map.199) | data formatting | bytes 98304

commit v5 on v4

--- a/solution.py
+++ b/solution.py
@@ -37,7 +37,7 @@
 def layer_kernel(n_sp, n_tp, *refs):
     (qa_h, ka_h, va_h, qb_h, kb_h, vb_h, sa_h, sb_h, oa_h, ob_h, resid_h, mg_h, fg_h, routes_h, gates_h,
      eg, eu, ed_h, sg_h, su_h, sd_h, out,
-     qa, ka, va, qb, kb, vb, sa, sb, oa, ob, resid, mg, fg, routes, gates, ed, sg, su, sd,
+     qa, ka, va, qb, kb, vb, sa, sb, oab, resid, mg, fg, routes, gates, ed, sg, su, sd,
      buf, accn, accf, ln, later,
      part, rs, sts, st, dsp_out, dsp_in, ret_out, ret_in, shp, shr, shs, shh, xbuf, xin, wgu, hs, hin, obuf, oh,
      choose, smat, rmat,
@@ -55,8 +55,9 @@
     wide = 2 * LANES
     nz = n_sp // 2
     up_steps = nz // 2
-    down_steps = nz - 1 - up_steps
-    last_far = nz - 2 - up_steps
+    down_steps = nz - up_steps
+    ups = (up_steps, up_steps, nz - 1 - down_steps, nz - 1 - down_steps)
+    downs = tuple(nz - 1 - n for n in ups)
     sp = lax.axis_index("sp")
     tp = lax.axis_index("tp")
     z = sp // 2
@@ -87,7 +88,7 @@
 
     staged = [
         (ka_h, ka), (va_h, va), (kb_h, kb), (vb_h, vb), (routes_h, routes), (qa_h, qa), (qb_h, qb), (sa_h, sa),
-        (sb_h, sb), (oa_h, oa), (ob_h, ob), (resid_h, resid), (mg_h, mg), (fg_h, fg), (gates_h, gates),
+        (sb_h, sb), (oa_h, oab.at[:LANES]), (ob_h, oab.at[LANES:]), (resid_h, resid), (mg_h, mg), (fg_h, fg), (gates_h, gates),
         (ed_h, ed), (sg_h, sg), (su_h, su), (sd_h, sd)]
     loads = [pltpu.make_async_copy(a, b, lsem.at[i]) for i, (a, b) in enumerate(staged)]
     for load in loads:
@@ -130,32 +131,49 @@
     def landed(ref, sem):
         pltpu.make_async_copy(ref, ref, sem).wait()
 
-    def sends_up(step):
-        return (z < nz - 1) & (z + 1 - step >= 0)
-
-    def sends_down(step):
-        return (z + step - 1) % nz <= last_far
-
-    def gets_up(step):
-        return z - step >= 0
-
-    def gets_down(step):
-        return (z + step) % nz <= last_far
-
-    def far(step):
-        return z + step >= nz
+    def sends_up(step, a):
+        return (z < nz - 1) & (z + 1 - step >= 0) & (step <= ups[a])
+
+    def sends_down(step, a):
+        return ((z + step - 1) % nz <= downs[a] - 1) & (step <= downs[a])
+
+    def gets_up(step, a):
+        return (z - step >= 0) & (step <= ups[a])
+
+    def gets_down(step, a):
+        return ((z + step) % nz <= downs[a] - 1) & (step <= downs[a])
+
+    def far(step, a):
+        return (z + step >= nz) & (step <= downs[a])
 
     for a in range(4):
-        @pl.when(sends_up(1))
+        @pl.when(sends_up(1, a))
         def _(a=a):
             up_copy(1, a, srcs[a]).start()
 
-        @pl.when(sends_down(1))
+        @pl.when(sends_down(1, a))
         def _(a=a):
             down_copy(1, a, srcs[a]).start()
 
         pair_copy(0, z, a, srcs[a]).start()
         buf[z, a, mine, :] = srcs[a][...]
+
+    def after_tp(k):
+        return (tp + k) % n_tp
+
+    def before_tp(k):
+        return (tp + n_tp - k) % n_tp
+
+    def weights_copy(h, g):
+        src = (eg, eu)[h].at[g // quarters, :, pl.ds(pl.multiple_of((g % quarters) * LANES, LANES), LANES)]
+        dst = wgu.at[tp, :, pl.ds(h * LANES, LANES)]
+        return src, dst
+
+    def weights_remote(h, g):
+        src, dst = weights_copy(h, g)
+        return pltpu.make_async_remote_copy(
+            src_ref=src, dst_ref=dst, send_sem=wsend.at[h, g], recv_sem=wrecv.at[h, tp],
+            device_id=(sp, g), device_id_type=MESH)
 
     span = 2 * rows
     j = lax.broadcasted_iota(jnp.int32, (span, span), 0)
@@ -167,66 +185,52 @@
     def index_of(shape, dim):
         return lax.broadcasted_iota(jnp.int32, shape, dim).astype(F32)
 
-    i = index_of((local * part_used, LANES), 0)
-    e = jnp.floor((i + 0.5) * (1.0 / part_used))
-    i = i - part_used * e
-    g = jnp.floor((i + 0.5) * (1.0 / CAP))
-    seat = g * PADDED + e * CAP + (i - CAP * g)
-    smat[...] = (index_of((local * part_used, part_seats), 1) == seat[:, 0:1]).astype(BF)
-    i = index_of((part_seats, LANES), 0)
-    g = jnp.floor((i + 0.5) * (1.0 / PADDED))
-    i = i - PADDED * g
-    e = jnp.floor((i + 0.5) * (1.0 / CAP))
-    seat = jnp.where(e < local, e * part_used + g * CAP + (i - CAP * e), -1.0)
-    rmat[...] = (index_of((part_seats, local * part_used), 1) == seat[:, 0:1]).astype(BF)
-    loads[4].wait()
-    experts = local * n_sp
-    e_at = index_of((rows, experts), 1)
-    named_by = [column(routes, k) for k in range(2)]
-    named = [e_at == named_by[k][:, 0:1] for k in range(2)]
-    members = jnp.where(named[0] | named[1], 1.0, 0.0).astype(BF)
-    prior = dot((index_of((rows, rows), 1) < index_of((rows, rows), 0)).astype(BF), members)
-    hits = None
-    for k in range(2):
-        home = jnp.floor((named_by[k] + 0.5) * (1.0 / local))
-        rank = jnp.sum(jnp.where(named[k], prior, 0.0), axis=1, keepdims=True)
-        seat = home * PADDED + (named_by[k] - local * home) * CAP + rank
-        oh[k] = (index_of((rows, seats), 1) == seat[:, 0:1]).astype(BF)
-        tall = jnp.concatenate([seat, jnp.full((wide - rows, LANES), -1.0, F32)], axis=0)
-        hit = index_of((seats, wide), 0) == jnp.transpose(tall)[0:1, :]
-        hits = hit if hits is None else hits | hit
-    choose[...] = hits.astype(BF)
-
-
-    def after_tp(k):
-        return (tp + k) % n_tp
-
-    def before_tp(k):
-        return (tp + n_tp - k) % n_tp
-
-    def weights_copy(h, g):
-        src = (eg, eu)[h].at[g // quarters, :, pl.ds(pl.multiple_of((g % quarters) * LANES, LANES), LANES)]
-        dst = wgu.at[tp, :, pl.ds(h * LANES, LANES)]
-        return src, dst
-
-    def weights_remote(h, g):
-        src, dst = weights_copy(h, g)
-        return pltpu.make_async_remote_copy(
-            src_ref=src, dst_ref=dst, send_sem=wsend.at[h, g], recv_sem=wrecv.at[h, tp],
-            device_id=(sp, g), device_id_type=MESH)
-
-    pl.semaphore_wait(tokens.at[0], len(row))
-
-    @pl.loop(1, n_tp)
-    def _(k):
+    def exchange_weights():
+        pl.semaphore_wait(tokens.at[0], len(row))
+
+        @pl.loop(1, n_tp)
+        def _(k):
+            for h in range(2):
+                weights_remote(h, after_tp(k)).start()
+
         for h in range(2):
-            weights_remote(h, after_tp(k)).start()
-
-    for h in range(2):
-        src, dst = weights_copy(h, tp)
-        pltpu.make_async_copy(src, dst, wloc.at[h]).start()
-
-    for load in loads[5:]:
+            src, dst = weights_copy(h, tp)
+            pltpu.make_async_copy(src, dst, wloc.at[h]).start()
+
+    def seat_masks():
+        i = index_of((local * part_used, LANES), 0)
+        e = jnp.floor((i + 0.5) * (1.0 / part_used))
+        i = i - part_used * e
+        g = jnp.floor((i + 0.5) * (1.0 / CAP))
+        seat = g * PADDED + e * CAP + (i - CAP * g)
+        smat[...] = (index_of((local * part_used, part_seats), 1) == seat[:, 0:1]).astype(BF)
+        i = index_of((part_seats, LANES), 0)
+        g = jnp.floor((i + 0.5) * (1.0 / PADDED))
+        i = i - PADDED * g
+        e = jnp.floor((i + 0.5) * (1.0 / CAP))
+        seat = jnp.where(e < local, e * part_used + g * CAP + (i - CAP * e), -1.0)
+        rmat[...] = (index_of((part_seats, local * part_used), 1) == seat[:, 0:1]).astype(BF)
+
+    def seat_rows():
+        loads[4].wait()
+        experts = local * n_sp
+        e_at = index_of((rows, experts), 1)
+        named_by = [column(routes, k) for k in range(2)]
+        named = [e_at == named_by[k][:, 0:1] for k in range(2)]
+        members = jnp.where(named[0] | named[1], 1.0, 0.0).astype(BF)
+        prior = dot((index_of((rows, rows), 1) < index_of((rows, rows), 0)).astype(BF), members)
+        hits = None
+        for k in range(2):
+            home = jnp.floor((named_by[k] + 0.5) * (1.0 / local))
+            rank = jnp.sum(jnp.where(named[k], prior, 0.0), axis=1, keepdims=True)
+            seat = home * PADDED + (named_by[k] - local * home) * CAP + rank
+            oh[k] = (index_of((rows, seats), 1) == seat[:, 0:1]).astype(BF)
+            tall = jnp.concatenate([seat, jnp.full((wide - rows, LANES), -1.0, F32)], axis=0)
+            hit = index_of((seats, wide), 0) == jnp.transpose(tall)[0:1, :]
+            hits = hit if hits is None else hits | hit
+        choose[...] = hits.astype(BF)
+
+    for load in loads[5:9]:
         load.wait()
     pl.semaphore_wait(tokens.at[1], 2)
     pass_on(2, along(rounds[1]))
@@ -267,29 +271,29 @@
         accf[:, cols(g)] = jnp.exp(-total) * accf[:, cols(g)] + added
 
     def poll_up(step, a):
-        @pl.when(gets_up(step))
+        @pl.when(gets_up(step, a))
         def _():
             ref = place(z - step, a)
             landed(ref, rsu.at[step - 1, a])
 
-            @pl.when((step < up_steps) & (z < nz - 1))
+            @pl.when((step < ups[a]) & (z < nz - 1))
             def _():
                 up_copy(step + 1, a, ref).start()
 
             pair_copy(step, z - step, a, ref).start()
 
     def poll_down(step, a):
-        @pl.when((step <= down_steps) & gets_down(step))
+        @pl.when(gets_down(step, a))
         def _():
             block = (z + step) % nz
             ref = place(block, a)
             landed(ref, rsd.at[step - 1, a])
 
-            @pl.when(step < down_steps)
+            @pl.when(step < downs[a])
             def _():
                 down_copy(step + 1, a, ref).start()
 
-            @pl.when(far(step))
+            @pl.when(far(step, a))
             def _():
                 pair_copy(up_steps + step, block, a, ref).start()
 
@@ -313,23 +317,31 @@
     @pl.loop(2, up_steps + 1)
     def _(step):
         before = step - 1
+        for when, piece in ((2, exchange_weights), (3, seat_rows), (4, seat_masks)):
+            pl.when(step == when)(piece)
         for a in range(4):
             poll_up(step, a)
             poll_down(step, a)
             g = a // 2
             if a % 2 == 0:
-                @pl.when(gets_up(before))
+                @pl.when(gets_up(before, a))
                 def _():
                     near(g, before)
             else:
-                @pl.when(far(before))
+                @pl.when(far(before, a))
                 def _():
                     distant(g, before)
 
-    @pl.when(gets_up(up_steps))
+    @pl.when(gets_up(up_steps, 0))
     def _():
-        for g in range(2):
-            near(g, up_steps)
+        near(0, up_steps)
+
+    @pl.when(far(down_steps, 2))
+    def _():
+        distant(1, down_steps)
+
+    for load in loads[9:]:
+        load.wait()
 
     pl.semaphore_wait(tokens.at[len(rounds)], 2)
     att = (accn[...] + jnp.exp(-ln[...]) * accf[...]).astype(BF)
@@ -342,22 +354,22 @@
         @pl.loop(1, up_steps + 1)
         def _(step):
             for a in range(4):
-                @pl.when(sends_up(step))
+                @pl.when(sends_up(step, a))
                 def _():
                     up_copy(step, a, place(z + 1 - step, a)).wait_send()
 
-                @pl.when(gets_up(step))
+                @pl.when(gets_up(step, a))
                 def _():
                     pair_copy(step, z - step, a, place(z - step, a)).wait_send()
 
         @pl.loop(1, down_steps + 1)
         def _(step):
             for a in range(4):
-                @pl.when(sends_down(step))
+                @pl.when(sends_down(step, a))
                 def _():
                     down_copy(step, a, place((z + step - 1) % nz, a)).wait_send()
 
-                @pl.when(far(step))
+                @pl.when(far(step, a))
                 def _():
                     pair_copy(up_steps + step, z + step - nz, a, place(z + step - nz, a)).wait_send()
 
@@ -384,13 +396,11 @@
                 g = after_tp(k)
                 tp_copy(phase, g, src(g), dst).wait_send()
 
-    low, high = att[:, :LANES], att[:, LANES:]
-
     @pl.loop(1, n_tp + 1)
     def _(k):
         g = after_tp(k)
         strip = pl.ds(pl.multiple_of(g * LANES, LANES), LANES)
-        part[g] = (dot(low, oa[:, strip]) + dot(high, ob[:, strip])).astype(BF)
+        part[g] = dot(att, oab[:, strip]).astype(BF)
 
         @pl.when(k < n_tp)
         def _():
@@ -625,14 +635,15 @@
     parts = 2
     nz = n_sp // 2
     up_steps = nz // 2
-    down_steps = nz - 1 - up_steps
+    down_steps = nz - up_steps
     operands = (
         query_a, key_a, value_a, query_b, key_b, value_b, stop_a.T, stop_b.T, out_a, out_b, resid,
         mix_gain.reshape(1, -1), ffn_gain.reshape(1, -1), routes.T, gates.T, exp_gate, exp_up, exp_down, sh_gate,
         sh_up, sh_down)
     dma = pltpu.SemaphoreType.DMA
     vmem = pltpu.VMEM
-    held = [vmem(a.shape, a.dtype) for i, a in enumerate(operands) if i not in (15, 16)]
+    held = [vmem(a.shape, a.dtype) for i, a in enumerate(operands) if i not in (9, 15, 16)]
+    held[8] = vmem((2 * out_a.shape[0], out_a.shape[1]), BF)
     return pl.pallas_call(
         functools.partial(layer_kernel, n_sp, n_tp),
         out_shape=jax.ShapeDtypeStruct((rows, LANES), BF),
@@ -666,14 +677,14 @@
             vmem((seats, 2 * LANES), BF),
             vmem((local * used // parts, seats // parts), BF),
             vmem((seats // parts, local * used // parts), BF),
-            dma((len(held),)),
+            dma((len(held) + 1,)),
             pltpu.SemaphoreType.REGULAR(((nz // 4).bit_length() + 1,)),
             dma((up_steps, 4)),
             dma((up_steps, 4)),
             dma((down_steps, 4)),
             dma((down_steps, 4)),
-            dma((nz, 4)),
-            dma((nz, 4)),
+            dma((nz + 1, 4)),
+            dma((nz + 1, 4)),
             dma((2, n_tp)),
             dma((2, n_tp)),
             dma((2,)),

time: 122 us -> 121 us (level)
  no operation moved by 1% of the time
where the time goes in v5:
time: 121 us
  Pallas kernels  120 us (99%)
  local copies, waits for them, and re-layouts  1.42 us (1%)
    pallas_call x1, Pallas kernels, shards(): pl.pallas_call(functools.partial(layer_kernel, n_sp, n_tp), out_shape=jax...  120 us

profile of v5, /device:TPU:1, one launch (start us, length us, event | category | flops | bytes accessed | tf_op | source)
XLA Modules:
  0.0 121.2 jit_solution(1715742659105790485)
XLA Ops:
  0.0 119.8 %shard_map.199 = bf16[192,128]{1,0:T(8,128)(2,1)} custom-call(bf16[192,128]{1,0:T(8,128)(2,1)} %refs_0_.1, bf16[192,128]{1,0:T(8,128)(2,1)} %refs_1_.1, bf16[192,128]{1,0:T(8,128)(2,1)} %refs_2_.1, bf16[192,128]{1,0:T(8,128)(2,1)} %refs_3_.1, bf16[192,128]{1,0:T(8,128)(2,1)} %refs_4_.1, bf16[192,128]{1,0:T(8,128)(2,1)} %refs_5_.1, f32[2,192]{1,0:T(2,128)} %bitcast.6, ...), custom_call_target="tpu_custom_call" | custom-call | tf_op jit(solution)/shard_map/pallas_call | solution.py:647
  119.8 1.4 %copy.23 = bf16[192,128]{1,0:T(8,128)(2,1)} copy(bf16[192,128]{1,0:T(8,128)(2,1)} %shard_map.199) | data formatting | bytes 98304

commit v6 on v5

--- a/solution.py
+++ b/solution.py
@@ -110,22 +110,22 @@
     def place(block, a):
         return buf.at[block, a, mine, :]
 
-    def other(block, a):
-        return buf.at[block, a, theirs, :]
+    def twin(block, g, half):
+        return buf.at[block, 2 * g : 2 * g + 2, half, :]
 
     def up_copy(step, a, src):
         return pltpu.make_async_remote_copy(
-            src_ref=src, dst_ref=place(z + 1 - step, a), send_sem=ssu.at[step - 1, a], recv_sem=rsu.at[step - 1, a],
+            src_ref=src, dst_ref=place(z + 1 - step, a), send_sem=ssu.at[step - 1, a // 2], recv_sem=rsu.at[step - 1, a],
             device_id=up_id, device_id_type=MESH)
 
     def down_copy(step, a, src):
         return pltpu.make_async_remote_copy(
-            src_ref=src, dst_ref=place((z + step - 1) % nz, a), send_sem=ssd.at[step - 1, a],
+            src_ref=src, dst_ref=place((z + step - 1) % nz, a), send_sem=ssd.at[step - 1, a // 2],
             recv_sem=rsd.at[step - 1, a], device_id=down_id, device_id_type=MESH)
 
     def pair_copy(index, block, a, src):
         return pltpu.make_async_remote_copy(
-            src_ref=src, dst_ref=place(block, a), send_sem=ssp.at[index, a], recv_sem=rsp.at[index, a],
+            src_ref=src, dst_ref=place(block, a), send_sem=ssp.at[index, a // 2], recv_sem=rsp.at[index, a // 2],
             device_id=pair_id, device_id_type=MESH)
 
     def landed(ref, sem):
@@ -161,9 +161,6 @@
     def after_tp(k):
         return (tp + k) % n_tp
 
-    def before_tp(k):
-        return (tp + n_tp - k) % n_tp
-
     def weights_copy(h, g):
         src = (eg, eu)[h].at[g // quarters, :, pl.ds(pl.multiple_of((g % quarters) * LANES, LANES), LANES)]
         dst = wgu.at[tp, :, pl.ds(h * LANES, LANES)]
@@ -172,7 +169,7 @@
     def weights_remote(h, g):
         src, dst = weights_copy(h, g)
         return pltpu.make_async_remote_copy(
-            src_ref=src, dst_ref=dst, send_sem=wsend.at[h, g], recv_sem=wrecv.at[h, tp],
+            src_ref=src, dst_ref=dst, send_sem=wsend.at[0], recv_sem=wrecv.at[0],
             device_id=(sp, g), device_id_type=MESH)
 
     span = 2 * rows
@@ -257,16 +254,14 @@
 
     def near(g, step):
         block = z - step
-        for a in (2 * g, 2 * g + 1):
-            landed(other(block, a), rsp.at[step, a])
+        landed(twin(block, g, theirs), rsp.at[step, g])
         added, total = groups[g](block)
         accn[:, cols(g)] += jnp.exp(-ln[:, cols(g)]) * added
         ln[:, cols(g)] += total
 
     def distant(g, step):
         block = z + step - nz
-        for a in (2 * g, 2 * g + 1):
-            landed(other(block, a), rsp.at[up_steps + step, a])
+        landed(twin(block, g, theirs), rsp.at[up_steps + step, g])
         added, total = groups[g](block)
         accf[:, cols(g)] = jnp.exp(-total) * accf[:, cols(g)] + added
 
@@ -301,8 +296,7 @@
     key_at = lax.broadcasted_iota(jnp.int32, (rows, span), 1)
     valid = key_at < row_at
     for g in range(2):
-        for a in (2 * g, 2 * g + 1):
-            landed(other(z, a), rsp.at[0, a])
+        landed(twin(z, g, theirs), rsp.at[0, g])
         added, total = groups[g](z, valid)
         accn[:, cols(g)] = added
         ln[:, cols(g)] = total
@@ -348,53 +342,48 @@
 
     @drains.append
     def _():
-        for a in range(4):
-            pair_copy(0, z, a, srcs[a]).wait_send()
+        for g in range(2):
+            landed(twin(z, g, mine), ssp.at[0, g])
 
         @pl.loop(1, up_steps + 1)
         def _(step):
-            for a in range(4):
-                @pl.when(sends_up(step, a))
+            for g in range(2):
+                @pl.when(sends_up(step, 2 * g))
                 def _():
-                    up_copy(step, a, place(z + 1 - step, a)).wait_send()
-
-                @pl.when(gets_up(step, a))
+                    landed(twin(z + 1 - step, g, mine), ssu.at[step - 1, g])
+
+                @pl.when(gets_up(step, 2 * g))
                 def _():
-                    pair_copy(step, z - step, a, place(z - step, a)).wait_send()
+                    landed(twin(z - step, g, mine), ssp.at[step, g])
 
         @pl.loop(1, down_steps + 1)
         def _(step):
-            for a in range(4):
-                @pl.when(sends_down(step, a))
+            for g in range(2):
+                @pl.when(sends_down(step, 2 * g))
                 def _():
-                    down_copy(step, a, place((z + step - 1) % nz, a)).wait_send()
-
-                @pl.when(far(step, a))
+                    landed(twin((z + step - 1) % nz, g, mine), ssd.at[step - 1, g])
+
+                @pl.when(far(step, 2 * g))
                 def _():
-                    pair_copy(up_steps + step, z + step - nz, a, place(z + step - nz, a)).wait_send()
-
-        @pl.loop(1, n_tp)
-        def _(k):
-            for h in range(2):
-                weights_remote(h, after_tp(k)).wait_send()
+                    landed(twin(z + step - nz, g, mine), ssp.at[up_steps + step, g])
+
+        landed(wgu.at[: n_tp - 1], wsend.at[0])
 
     def tp_copy(phase, g, src, dst):
         return pltpu.make_async_remote_copy(
-            src_ref=src, dst_ref=dst, send_sem=tp_send.at[phase, g], recv_sem=tp_recv.at[phase, tp],
+            src_ref=src, dst_ref=dst, send_sem=tp_send.at[phase], recv_sem=tp_recv.at[phase],
             device_id=(sp, g), device_id_type=MESH)
 
-    def sp_copy(phase, d, src, dst):
+    def sp_copy(phase, d, src, dst, part_of=0):
         return pltpu.make_async_remote_copy(
-            src_ref=src, dst_ref=dst, send_sem=sp_send.at[phase, d], recv_sem=sp_recv.at[phase, sp],
+            src_ref=src, dst_ref=dst, send_sem=sp_send.at[phase], recv_sem=sp_recv.at[phase * parts + part_of],
             device_id=(d, tp), device_id_type=MESH)
 
-    def tp_drain(phase, src, dst):
-        @drains.append
-        def _():
-            @pl.loop(1, n_tp)
-            def _(k):
-                g = after_tp(k)
-                tp_copy(phase, g, src(g), dst).wait_send()
+    def from_all(ref, phase):
+        landed(ref.at[: n_tp - 1], tp_recv.at[phase])
+
+    def tp_drain(phase, ref):
+        drains.append(lambda: landed(ref, tp_send.at[phase]))
 
     @pl.loop(1, n_tp + 1)
     def _(k):
@@ -406,14 +395,17 @@
         def _():
             tp_copy(0, g, part.at[g], rs.at[tp]).start()
 
-    tp_drain(0, lambda g: part.at[g], rs.at[tp])
-
-    def gather_rs(k, total):
-        src = before_tp(k)
-        landed(rs.at[src], tp_recv.at[0, src])
-        return total + rs[src].astype(F32)
-
-    mixed = lax.fori_loop(1, n_tp, gather_rs, part[tp].astype(F32))
+    tp_drain(0, part.at[: n_tp - 1])
+
+    def added_up(ref):
+        total = ref[0].astype(F32)
+        for g in range(1, n_tp):
+            total = total + ref[g].astype(F32)
+        return total
+
+    rs[tp] = part[tp]
+    from_all(rs, 0)
+    mixed = added_up(rs)
 
     gained = mixed * mg[...]
     x = resid[...].astype(F32)
@@ -428,14 +420,11 @@
     def _(k):
         tp_copy(1, after_tp(k), sts, st.at[tp]).start()
 
-    tp_drain(1, lambda g: sts, st.at[tp])
-
-    def gather_st(k, total):
-        src = before_tp(k)
-        landed(st.at[src], tp_recv.at[1, src])
-        return total + st[src]
-
-    lines = lax.fori_loop(1, n_tp, gather_st, lines)
+    tp_drain(1, st.at[: n_tp - 1])
+
+    st[tp] = lines
+    from_all(st, 1)
+    lines = added_up(st)
     total = jnp.transpose(jnp.concatenate([lines, jnp.zeros((LANES - 8, wide), F32)], axis=0))[:rows, :]
     scale = lax.rsqrt(total[:, 0:1] / D + EPS)
     square = total[:, 1:2] + scale * (2.0 * total[:, 2:3] + scale * total[:, 3:4])
@@ -464,10 +453,10 @@
         return 2 * ((z + nz - nz // 4 + place // 2) % nz) + place % 2
 
     def dispatch(d):
-        return sp_copy(0, d, dsp_out.at[d], dsp_in.at[berth(sp, d)])
+        return sp_copy(0, d, dsp_out.at[d], dsp_in.at[berth(sp, d)], berth(sp, d) // homes)
 
     near_first(lambda d: dispatch(d).start())
-    drains.append(lambda: near_first(lambda d: dispatch(d).wait_send()))
+    drains.append(lambda: landed(dsp_out.at[: n_sp - 1], sp_send.at[0]))
     dsp_in[berth(sp, sp)] = dsp_out[sp]
 
     shp[:, :, :units] = dot(normed, sg[...]).reshape(strips, 16, units).astype(BF)
@@ -483,17 +472,14 @@
 
     @drains.append
     def _():
-        @pl.loop(1, n_tp)
-        def _(k):
-            g = after_tp(k)
-
-            @pl.when(g < strips)
-            def _():
-                tp_copy(2, g, shp.at[g], shr.at[tp]).wait_send()
-
-            @pl.when(tp < strips)
-            def _():
-                tp_copy(3, g, shs, shh.at[tp]).wait_send()
+        @pl.when(tp < strips)
+        def _():
+            landed(shp.at[: strips - 1], tp_send.at[2])
+            landed(shr.at[: n_tp - 1, :, :units], tp_send.at[3])
+
+        @pl.when(tp >= strips)
+        def _():
+            landed(shp, tp_send.at[2])
 
     def gated(gate, up):
         return (gate / (1.0 + jnp.exp(-gate)) * up).astype(BF)
@@ -501,12 +487,9 @@
     def reduce_shared():
         @pl.when(tp < strips)
         def _():
-            def gather(k, total):
-                src = before_tp(k)
-                landed(shr.at[src], tp_recv.at[2, src])
-                return total + shr[src].astype(F32)
-
-            both = lax.fori_loop(1, n_tp, gather, shp[tp].astype(F32))
+            shr[tp] = shp[tp]
+            from_all(shr, 2)
+            both = added_up(shr)
             hidden = gated(both[:, :units], both[:, units:])
             shs[...] = hidden
             shh[tp] = hidden
@@ -516,14 +499,8 @@
                 tp_copy(3, after_tp(k), shs, shh.at[tp]).start()
 
     def send_rows(p):
-        @pl.loop(p * homes, (p + 1) * homes)
-        def _(place):
-            src = tenant(place)
-
-            @pl.when(src != sp)
-            def _():
-                landed(dsp_in.at[place], sp_recv.at[0, src])
-
+        first_one = p * homes if p else 1
+        landed(dsp_in.at[first_one : (p + 1) * homes], sp_recv.at[p])
         flat = dsp_in[p * homes : (p + 1) * homes].astype(F32).reshape(part_seats, LANES).astype(BF)
         xbuf[p] = dot(smat[...], flat).reshape(local, part_used, LANES).astype(BF)
         xin[p, tp] = xbuf[p, tp // quarters]
@@ -533,14 +510,10 @@
             g = after_tp(k)
             tp_copy(4 + p, g, xbuf.at[p, g // quarters], xin.at[p, tp]).start()
 
-        tp_drain(4 + p, lambda g: xbuf.at[p, g // quarters], xin.at[p, tp])
+        tp_drain(4 + p, xin.at[p, : n_tp - 1])
 
     def send_hidden(p):
-        @pl.loop(1, n_tp)
-        def _(k):
-            src = before_tp(k)
-            landed(xin.at[p, src], tp_recv.at[4 + p, src])
-
+        from_all(xin.at[p], 4 + p)
         x = jnp.concatenate([xin[p, g] for g in range(n_tp)], axis=1)
         both = dot(x, wgu[...].reshape(n_tp * LANES, 2 * LANES))
         hidden = gated(both[:, :LANES], both[:, LANES:])
@@ -551,18 +524,14 @@
         def _(k):
             tp_copy(4 + parts + p, after_tp(k), hs.at[p], hin.at[p, tp]).start()
 
-        tp_drain(4 + parts + p, lambda g: hs.at[p], hin.at[p, tp])
+        tp_drain(4 + parts + p, hin.at[p, : n_tp - 1])
 
     def giving(place):
         d = tenant(place)
         return sp_copy(1, d, ret_out.at[place], ret_in.at[sp])
 
     def send_back(p):
-        @pl.loop(1, n_tp)
-        def _(k):
-            src = before_tp(k)
-            landed(hin.at[p, src], tp_recv.at[4 + parts + p, src])
-
+        from_all(hin.at[p], 4 + parts + p)
         for e in range(local):
             h = jnp.concatenate([hin[p, quarters * e + q] for q in range(quarters)], axis=1)
             obuf[e * part_used : (e + 1) * part_used, :] = dot(h, ed[e]).astype(BF)
@@ -575,13 +544,7 @@
             def _():
                 giving(place).start()
 
-    @drains.append
-    def _():
-        @pl.loop(0, n_sp)
-        def _(place):
-            @pl.when(tenant(place) != sp)
-            def _():
-                giving(place).wait_send()
+    drains.append(lambda: landed(ret_out.at[: n_sp - 1], sp_send.at[1]))
 
     send_rows(0)
     reduce_shared()
@@ -589,12 +552,7 @@
         src, dst = weights_copy(h, tp)
         pltpu.make_async_copy(src, dst, wloc.at[h]).wait()
 
-    @pl.loop(1, n_tp)
-    def _(k):
-        src = before_tp(k)
-        for h in range(2):
-            landed(wgu.at[src, :, pl.ds(h * LANES, LANES)], wrecv.at[h, src])
-
+    landed(wgu.at[: n_tp - 1], wrecv.at[0])
     for p in range(1, parts):
         send_rows(p)
         send_hidden(p - 1)
@@ -604,19 +562,17 @@
     ret_in[sp] = ret_out[berth(sp, sp)]
     weights = [column(gates, k) for k in range(2)]
 
-    @pl.loop(0, strips)
-    def _(src):
-        @pl.when(src != tp)
-        def _():
-            landed(shh.at[src], tp_recv.at[3, src])
+    @pl.when(tp < strips)
+    def _():
+        landed(shh.at[: strips - 1], tp_recv.at[3])
+
+    @pl.when(tp >= strips)
+    def _():
+        landed(shh, tp_recv.at[3])
 
     shared_out = dot(shh[...].reshape(rows, units), sd[...])
 
-    @pl.loop(1, n_sp)
-    def _(k):
-        src = (sp + n_sp - k) % n_sp
-        landed(ret_in.at[src], sp_recv.at[1, src])
-
+    landed(ret_in.at[: n_sp - 1], sp_recv.at[parts])
     flat = ret_in[...].astype(F32).reshape(seats, LANES).astype(BF)
     routed = weights[0] * dot(oh[0], flat) + weights[1] * dot(oh[1], flat)
     out[...] = (stream + (routed + shared_out)).astype(BF)
@@ -679,19 +635,19 @@
             vmem((seats // parts, local * used // parts), BF),
             dma((len(held) + 1,)),
             pltpu.SemaphoreType.REGULAR(((nz // 4).bit_length() + 1,)),
+            dma((up_steps, 2)),
             dma((up_steps, 4)),
-            dma((up_steps, 4)),
+            dma((down_steps, 2)),
             dma((down_steps, 4)),
-            dma((down_steps, 4)),
-            dma((nz + 1, 4)),
-            dma((nz + 1, 4)),
-            dma((2, n_tp)),
-            dma((2, n_tp)),
+            dma((nz + 1, 2)),
+            dma((nz + 1, 2)),
+            dma((1,)),
+            dma((1,)),
             dma((2,)),
-            dma((4 + 2 * parts, n_tp)),
-            dma((4 + 2 * parts, n_tp)),
-            dma((2, n_sp)),
-            dma((2, n_sp)),
+            dma((4 + 2 * parts,)),
+            dma((4 + 2 * parts,)),
+            dma((2,)),
+            dma((parts + 1,)),
         ],
         compiler_params=pltpu.CompilerParams(
             collective_id=0, has_side_effects=True, vmem_limit_bytes=56 * 1024 * 1024),

time: 121 us -> 114 us (0.942)
  Pallas kernels: 120 us -> 112 us
    pallas_call x1, Pallas kernels: 120 us -> 112 us  [shards(): pl.pallas_call(functools.partial(layer_kernel, n_sp, n_tp), out_shape=jax...]
where the time goes in v6:
time: 114 us
  Pallas kernels  112 us (98%)
  local copies, waits for them, and re-layouts  1.42 us (1%)
    pallas_call x1, Pallas kernels, shards(): pl.pallas_call(functools.partial(layer_kernel, n_sp, n_tp), out_shape=jax...  112 us

profile of v6, /device:TPU:1, one launch (start us, length us, event | category | flops | bytes accessed | tf_op | source)
XLA Modules:
  0.0 113.9 jit_solution(5847724844595596001)
XLA Ops:
  0.0 112.5 %shard_map.199 = bf16[192,128]{1,0:T(8,128)(2,1)} custom-call(bf16[192,128]{1,0:T(8,128)(2,1)} %refs_0_.1, bf16[192,128]{1,0:T(8,128)(2,1)} %refs_1_.1, bf16[192,128]{1,0:T(8,128)(2,1)} %refs_2_.1, bf16[192,128]{1,0:T(8,128)(2,1)} %refs_3_.1, bf16[192,128]{1,0:T(8,128)(2,1)} %refs_4_.1, bf16[192,128]{1,0:T(8,128)(2,1)} %refs_5_.1, f32[2,192]{1,0:T(2,128)} %bitcast.6, ...), custom_call_target="tpu_custom_call" | custom-call | tf_op jit(solution)/shard_map/pallas_call | solution.py:603
  112.5 1.4 %copy.23 = bf16[192,128]{1,0:T(8,128)(2,1)} copy(bf16[192,128]{1,0:T(8,128)(2,1)} %shard_map.199) | data formatting | bytes 98304

commit v7 on v6

--- a/solution.py
+++ b/solution.py
@@ -48,6 +48,7 @@
     used = n_sp * CAP
     seats = n_sp * PADDED
     parts = 2
+    filled = local * CAP
     part_used = used // parts
     part_seats = seats // parts
     homes = n_sp // parts
@@ -67,6 +68,9 @@
     pair_id = (2 * z + 1 - c, tp)
     drains = []
 
+    dsp_in[...] = jnp.zeros_like(dsp_in)
+    ret_in[...] = jnp.zeros_like(ret_in)
+    st[...] = jnp.zeros_like(st)
     barrier = pltpu.get_barrier_semaphore()
 
     side = quarters
@@ -418,12 +422,12 @@
 
     @pl.loop(1, n_tp)
     def _(k):
-        tp_copy(1, after_tp(k), sts, st.at[tp]).start()
-
-    tp_drain(1, st.at[: n_tp - 1])
+        tp_copy(1, after_tp(k), sts.at[:4], st.at[tp, :4]).start()
+
+    tp_drain(1, st.at[: n_tp - 1, :4])
 
     st[tp] = lines
-    from_all(st, 1)
+    landed(st.at[: n_tp - 1, :4], tp_recv.at[1])
     lines = added_up(st)
     total = jnp.transpose(jnp.concatenate([lines, jnp.zeros((LANES - 8, wide), F32)], axis=0))[:rows, :]
     scale = lax.rsqrt(total[:, 0:1] / D + EPS)
@@ -435,9 +439,10 @@
     tall = jnp.concatenate([normed, jnp.zeros((wide - rows, LANES), BF)], axis=0)
     dsp_out[...] = dot(choose[...], tall).reshape(n_sp, PADDED, LANES).astype(BF)
 
-    def near_first(body):
+    def far_first(body):
         @pl.loop(0, nz)
-        def _(k):
+        def _(turn):
+            k = nz - 1 - turn
             reach = (k + 1) // 2
             away = (z + nz + reach * (2 * (k % 2) - 1)) % nz
             body(2 * away + 1 - c)
@@ -453,10 +458,10 @@
         return 2 * ((z + nz - nz // 4 + place // 2) % nz) + place % 2
 
     def dispatch(d):
-        return sp_copy(0, d, dsp_out.at[d], dsp_in.at[berth(sp, d)], berth(sp, d) // homes)
-
-    near_first(lambda d: dispatch(d).start())
-    drains.append(lambda: landed(dsp_out.at[: n_sp - 1], sp_send.at[0]))
+        return sp_copy(0, d, dsp_out.at[d, :filled], dsp_in.at[berth(sp, d), :filled], berth(sp, d) // homes)
+
+    far_first(lambda d: dispatch(d).start())
+    drains.append(lambda: landed(dsp_out.at[: n_sp - 1, :filled], sp_send.at[0]))
     dsp_in[berth(sp, sp)] = dsp_out[sp]
 
     shp[:, :, :units] = dot(normed, sg[...]).reshape(strips, 16, units).astype(BF)
@@ -500,7 +505,7 @@
 
     def send_rows(p):
         first_one = p * homes if p else 1
-        landed(dsp_in.at[first_one : (p + 1) * homes], sp_recv.at[p])
+        landed(dsp_in.at[first_one : (p + 1) * homes, :filled], sp_recv.at[p])
         flat = dsp_in[p * homes : (p + 1) * homes].astype(F32).reshape(part_seats, LANES).astype(BF)
         xbuf[p] = dot(smat[...], flat).reshape(local, part_used, LANES).astype(BF)
         xin[p, tp] = xbuf[p, tp // quarters]
@@ -528,7 +533,7 @@
 
     def giving(place):
         d = tenant(place)
-        return sp_copy(1, d, ret_out.at[place], ret_in.at[sp])
+        return sp_copy(1, d, ret_out.at[place, :filled], ret_in.at[sp, :filled])
 
     def send_back(p):
         from_all(hin.at[p], 4 + parts + p)
@@ -544,20 +549,20 @@
             def _():
                 giving(place).start()
 
-    drains.append(lambda: landed(ret_out.at[: n_sp - 1], sp_send.at[1]))
-
-    send_rows(0)
+    drains.append(lambda: landed(ret_out.at[: n_sp - 1, :filled], sp_send.at[1]))
+
+    send_rows(parts - 1)
     reduce_shared()
     for h in range(2):
         src, dst = weights_copy(h, tp)
         pltpu.make_async_copy(src, dst, wloc.at[h]).wait()
 
     landed(wgu.at[: n_tp - 1], wrecv.at[0])
-    for p in range(1, parts):
+    for p in reversed(range(parts - 1)):
         send_rows(p)
-        send_hidden(p - 1)
-    send_hidden(parts - 1)
-    for p in range(parts):
+        send_hidden(p + 1)
+    send_hidden(0)
+    for p in reversed(range(parts)):
         send_back(p)
     ret_in[sp] = ret_out[berth(sp, sp)]
     weights = [column(gates, k) for k in range(2)]
@@ -572,7 +577,7 @@
 
     shared_out = dot(shh[...].reshape(rows, units), sd[...])
 
-    landed(ret_in.at[: n_sp - 1], sp_recv.at[parts])
+    landed(ret_in.at[: n_sp - 1, :filled], sp_recv.at[parts])
     flat = ret_in[...].astype(F32).reshape(seats, LANES).astype(BF)
     routed = weights[0] * dot(oh[0], flat) + weights[1] * dot(oh[1], flat)
     out[...] = (stream + (routed + shared_out)).astype(BF)

time: 114 us -> 111 us (0.974)
  Pallas kernels: 112 us -> 109 us
    pallas_call x1, Pallas kernels: 112 us -> 109 us  [shards(): pl.pallas_call(functools.partial(layer_kernel, n_sp, n_tp), out_shape=jax...]
where the time goes in v7:
time: 111 us; the launch traced here: 110 us
  Pallas kernels  109 us (98%)
  local copies, waits for them, and re-layouts  1.42 us (1%)
    pallas_call x1, Pallas kernels, shards(): pl.pallas_call(functools.partial(layer_kernel, n_sp, n_tp), out_shape=jax...  109 us

profile of v7, /device:TPU:1, one launch (start us, length us, event | category | flops | bytes accessed | tf_op | source)
XLA Modules:
  0.0 110.4 jit_solution(9289435894806549345)
XLA Ops:
  0.0 109.0 %shard_map.199 = bf16[192,128]{1,0:T(8,128)(2,1)} custom-call(bf16[192,128]{1,0:T(8,128)(2,1)} %refs_0_.1, bf16[192,128]{1,0:T(8,128)(2,1)} %refs_1_.1, bf16[192,128]{1,0:T(8,128)(2,1)} %refs_2_.1, bf16[192,128]{1,0:T(8,128)(2,1)} %refs_3_.1, bf16[192,128]{1,0:T(8,128)(2,1)} %refs_4_.1, bf16[192,128]{1,0:T(8,128)(2,1)} %refs_5_.1, f32[2,192]{1,0:T(2,128)} %bitcast.6, ...), custom_call_target="tpu_custom_call" | custom-call | tf_op jit(solution)/shard_map/pallas_call | solution.py:608
  109.0 1.4 %copy.23 = bf16[192,128]{1,0:T(8,128)(2,1)} copy(bf16[192,128]{1,0:T(8,128)(2,1)} %shard_map.199) | data formatting | bytes 98304

commit v8 on v7

--- a/solution.py
+++ b/solution.py
@@ -389,15 +389,19 @@
     def tp_drain(phase, ref):
         drains.append(lambda: landed(ref, tp_send.at[phase]))
 
-    @pl.loop(1, n_tp + 1)
-    def _(k):
-        g = after_tp(k)
+    def hops(offset):
+        return sum(min(n, side - n) for n in divmod(offset, side))
+
+    offsets = sorted(range(1, n_tp), key=hops, reverse=True)
+    owners = [(tp // side + o // side) % side * side + (tp + o) % side for o in offsets]
+
+    def project(g):
         strip = pl.ds(pl.multiple_of(g * LANES, LANES), LANES)
-        part[g] = dot(att, oab[:, strip]).astype(BF)
-
-        @pl.when(k < n_tp)
-        def _():
-            tp_copy(0, g, part.at[g], rs.at[tp]).start()
+        return dot(att, oab[:, strip]).astype(BF)
+
+    for g in owners:
+        part[g] = project(g)
+        tp_copy(0, g, part.at[g], rs.at[tp]).start()
 
     tp_drain(0, part.at[: n_tp - 1])
 
@@ -407,7 +411,7 @@
             total = total + ref[g].astype(F32)
         return total
 
-    rs[tp] = part[tp]
+    rs[tp] = project(tp)
     from_all(rs, 0)
     mixed = added_up(rs)
 
@@ -420,9 +424,8 @@
     lines = jnp.transpose(jnp.concatenate([own, jnp.zeros((wide - rows, LANES), F32)], axis=0))[0:8, :]
     sts[...] = lines
 
-    @pl.loop(1, n_tp)
-    def _(k):
-        tp_copy(1, after_tp(k), sts.at[:4], st.at[tp, :4]).start()
+    for g in owners:
+        tp_copy(1, g, sts.at[:4], st.at[tp, :4]).start()
 
     tp_drain(1, st.at[: n_tp - 1, :4])
 
@@ -467,12 +470,9 @@
     shp[:, :, :units] = dot(normed, sg[...]).reshape(strips, 16, units).astype(BF)
     shp[:, :, units:] = dot(normed, su[...]).reshape(strips, 16, units).astype(BF)
 
-    @pl.loop(1, n_tp)
-    def _(k):
-        g = after_tp(k)
-
+    for g in owners:
         @pl.when(g < strips)
-        def _():
+        def _(g=g):
             tp_copy(2, g, shp.at[g], shr.at[tp]).start()
 
     @drains.append
@@ -499,9 +499,8 @@
             shs[...] = hidden
             shh[tp] = hidden
 
-            @pl.loop(1, n_tp)
-            def _(k):
-                tp_copy(3, after_tp(k), shs, shh.at[tp]).start()
+            for g in owners:
+                tp_copy(3, g, shs, shh.at[tp]).start()
 
     def send_rows(p):
         first_one = p * homes if p else 1
@@ -510,9 +509,7 @@
         xbuf[p] = dot(smat[...], flat).reshape(local, part_used, LANES).astype(BF)
         xin[p, tp] = xbuf[p, tp // quarters]
 
-        @pl.loop(1, n_tp)
-        def _(k):
-            g = after_tp(k)
+        for g in owners:
             tp_copy(4 + p, g, xbuf.at[p, g // quarters], xin.at[p, tp]).start()
 
         tp_drain(4 + p, xin.at[p, : n_tp - 1])
@@ -525,9 +522,8 @@
         hs[p] = hidden
         hin[p, tp] = hidden
 
-        @pl.loop(1, n_tp)
-        def _(k):
-            tp_copy(4 + parts + p, after_tp(k), hs.at[p], hin.at[p, tp]).start()
+        for g in owners:
+            tp_copy(4 + parts + p, g, hs.at[p], hin.at[p, tp]).start()
 
         tp_drain(4 + parts + p, hin.at[p, : n_tp - 1])
 
@@ -552,7 +548,6 @@
     drains.append(lambda: landed(ret_out.at[: n_sp - 1, :filled], sp_send.at[1]))
 
     send_rows(parts - 1)
-    reduce_shared()
     for h in range(2):
         src, dst = weights_copy(h, tp)
         pltpu.make_async_copy(src, dst, wloc.at[h]).wait()
@@ -561,6 +556,7 @@
     for p in reversed(range(parts - 1)):
         send_rows(p)
         send_hidden(p + 1)
+    reduce_shared()
     send_hidden(0)
     for p in reversed(range(parts)):
         send_back(p)
@@ -607,7 +603,7 @@
     held[8] = vmem((2 * out_a.shape[0], out_a.shape[1]), BF)
     return pl.pallas_call(
         functools.partial(layer_kernel, n_sp, n_tp),
-        out_shape=jax.ShapeDtypeStruct((rows, LANES), BF),
+        out_shape=pltpu.VMEM((rows, LANES), BF),
         in_specs=[pl.BlockSpec(memory_space=pl.ANY)] * len(operands),
         out_specs=pl.BlockSpec(memory_space=pltpu.VMEM),
         scratch_shapes=held + [

time: 111 us -> 107 us (0.964)
  Pallas kernels: 109 us -> 106 us
    pallas_call x1, Pallas kernels: 109 us -> 106 us  [shards(): pl.pallas_call(functools.partial(layer_kernel, n_sp, n_tp), out_shape=plt...]
where the time goes in v8:
time: 107 us
  Pallas kernels  106 us (99%)
    pallas_call x1, Pallas kernels, shards(): pl.pallas_call(functools.partial(layer_kernel, n_sp, n_tp), out_shape=plt...  106 us

profile of v8, /device:TPU:1, one launch (start us, length us, event | category | flops | bytes accessed | tf_op | source)
XLA Modules:
  0.0 106.9 jit_solution(18176213249324515593)
XLA Ops:
  0.0 106.2 %shard_map.199 = bf16[192,128]{1,0:T(8,128)(2,1)S(1)} custom-call(bf16[192,128]{1,0:T(8,128)(2,1)} %refs_0_.1, bf16[192,128]{1,0:T(8,128)(2,1)} %refs_1_.1, bf16[192,128]{1,0:T(8,128)(2,1)} %refs_2_.1, bf16[192,128]{1,0:T(8,128)(2,1)} %refs_3_.1, bf16[192,128]{1,0:T(8,128)(2,1)} %refs_4_.1, bf16[192,128]{1,0:T(8,128)(2,1)} %refs_5_.1, f32[2,192]{1,0:T(2,128)} %bitcast.6, ...), custom_call_target="tpu_custom_call" | custom-call | tf_op jit(solution)/shard_map/pallas_call | solution.py:604
  106.2 0.6 copy.23
